TPU v7x, 32 devices: a whole 2x2x4 slice. The times are simulated.
32 devices in a mesh: sp: 8 (over z, x), tp: 4 (over y, core).
Axes of the slice: x: 2, y: 2, z: 4, core: 2. Of those that a mesh axis runs over, the one named last changes fastest.
Arguments:
- tokens: bfloat16 [8192, 2048], P('sp', 'tp'), may hold values from -70 to 70
- w_query: bfloat16 [2048, 1024], P(None, 'tp'), may hold values from -0.125 to 0.125
- w_key: bfloat16 [2048, 1024], P(None, 'tp'), may hold values from -0.125 to 0.125
- w_value: bfloat16 [2048, 1024], P(None, 'tp'), may hold values from -0.125 to 0.125
- w_delta_gate: bfloat16 [2048, 1024], P(None, 'tp'), may hold values from -0.125 to 0.125
- w_glu_value: bfloat16 [2048, 1024], P(None, 'tp'), may hold values from -0.125 to 0.125
- w_glu_gate: bfloat16 [2048, 1024], P(None, 'tp'), may hold values from -0.125 to 0.125
- w_conv_gate: bfloat16 [2048, 1024], P(None, 'tp'), may hold values from -0.125 to 0.125
- w_beta: bfloat16 [2048, 8], replicated, may hold values from -0.125 to 0.125
- w_decay: bfloat16 [2048, 8], replicated, may hold values from -0.125 to 0.125
- decay_log: float32 [8], replicated, may hold values from -12 to -3
- head_gain: float32 [128], replicated, may hold values from 0.1 to 1.9
- conv_taps: bfloat16 [31, 1024], P(None, 'tp'), may hold values from -2.5 to 2.5
- ln_gain: float32 [1024], P('tp'), may hold values from 0.1 to 1.9
- ln_shift: float32 [1024], P('tp'), may hold values from -3 to 3
- out_delta: bfloat16 [1024, 2048], P('tp'), may hold values from -0.125 to 0.125
- out_conv: bfloat16 [1024, 2048], P('tp'), may hold values from -0.125 to 0.125
Outputs:
- mixed_out: bfloat16 [8192, 2048], P(('sp', 'tp'))
All inputs are finite; a program needn't handle non-finite values.
Results may differ from a plain program's by a relative error of at most 0.024.
Values may be sent and summed in bfloat16 or wider, within the bound.
A program may use at most 64 MiB of HBM per device.

v0:
```python
import jax
import jax.numpy as jnp
from jax import lax
from jax.sharding import PartitionSpec as P

SPAN = 64


TINY_NORM = 1e-06
TINY_VAR = 1e-05
HIGHEST = lax.Precision.HIGHEST


def entering(part, axis, combine, identity):
    place = lax.axis_index(axis)
    gathered = lax.all_gather(part, axis)
    state = jnp.zeros_like(part) + jnp.asarray(identity, part.dtype)

    def one(hop, state):
        return combine(state, lax.dynamic_index_in_dim(gathered, hop, 0, False))

    return lax.fori_loop(0, place, one, state)


def shifted(block, axis, distance):
    devices = range(lax.axis_size(axis))
    route = [(i - distance, i) for i in devices if i - distance in devices]
    return lax.ppermute(block, axis, route)


def block_terms(query, keys, values, strength, log_decay):
    log_sum = jnp.cumsum(log_decay, axis=-1)
    offsets = jnp.arange(SPAN)
    causal = offsets[:, None] >= offsets[None, :]
    strict = offsets[:, None] > offsets[None, :]
    spread = log_sum[..., :, None] - log_sum[..., None, :]
    damping = jnp.where(causal, jnp.exp(jnp.where(causal, spread, 0.0)), 0.0)
    scaled_keys = keys * strength[..., None]
    lower = jnp.where(
        strict, jnp.einsum("hnid,hnjd->hnij", scaled_keys, keys, precision=HIGHEST) * damping, 0.0
    )
    identity = jnp.eye(SPAN, dtype=jnp.float32)
    right = jnp.concatenate(
        [values * strength[..., None], scaled_keys * jnp.exp(log_sum)[..., None]], axis=-1
    )
    solved = jax.scipy.linalg.solve_triangular(
        identity + lower, right, lower=True, unit_diagonal=True
    )
    width = values.shape[-1]
    scores = jnp.einsum("hnid,hnjd->hnij", query, keys, precision=HIGHEST) * damping
    return (log_sum, solved[..., :width], solved[..., width:], scores)


def local(
    tokens,
    w_query,
    w_key,
    w_value,
    w_delta_gate,
    w_glu_value,
    w_glu_gate,
    w_conv_gate,
    w_beta,
    w_decay,
    decay_log,
    head_gain,
    conv_taps,
    ln_gain,
    ln_shift,
    out_delta,
    out_conv,
):
    rows_here = tokens.shape[0]
    tp_size = lax.axis_size("tp")
    width_all = tokens.shape[1] * tp_size
    weights = (
        w_query,
        w_key,
        w_value,
        w_delta_gate,
        w_glu_value,
        w_glu_gate,
        w_conv_gate,
        w_beta,
        w_decay,
    )
    piece = lax.all_gather(tokens, "tp", axis=1, tiled=True)
    totals = tuple(
        (jnp.dot(piece, weight, preferred_element_type=jnp.float32) for weight in weights)
    )
    squares = jnp.sum(jnp.square(piece.astype(jnp.float32)), axis=1)
    sums, squares = (totals, squares)
    inv_rms = lax.rsqrt(squares / width_all + TINY_NORM)[:, None]
    scaled = [summed * inv_rms for summed in sums]
    query_raw, key_raw, value_raw, delta_gate_raw, glu_value_raw, glu_gate_raw, conv_gate_raw = [
        item.astype(jnp.bfloat16) for item in scaled[:7]
    ]
    head_size = head_gain.shape[0]
    heads_here = w_query.shape[1] // head_size
    first_head = lax.axis_index("tp") * heads_here
    strength = jax.nn.sigmoid(lax.dynamic_slice_in_dim(scaled[7], first_head, heads_here, 1))
    rates = jnp.exp(lax.dynamic_slice_in_dim(decay_log, first_head, heads_here, 0))
    log_decay = -rates[None, :] * jax.nn.softplus(
        lax.dynamic_slice_in_dim(scaled[8], first_head, heads_here, 1)
    )
    blocks = rows_here // SPAN

    def to_blocks(raw):
        return jnp.transpose(raw.reshape(blocks, SPAN, heads_here, head_size), (2, 0, 1, 3))

    def unit_rows(array):
        return array * lax.rsqrt(jnp.sum(array * array, axis=-1, keepdims=True) + TINY_NORM)

    query = unit_rows(to_blocks(query_raw.astype(jnp.float32))) * head_size ** (-0.5)
    keys = unit_rows(to_blocks(key_raw.astype(jnp.float32)))
    values = to_blocks(value_raw.astype(jnp.float32))
    strength_blocks = jnp.transpose(strength.reshape(blocks, SPAN, heads_here), (2, 0, 1))
    decay_blocks = jnp.transpose(log_decay.reshape(blocks, SPAN, heads_here), (2, 0, 1))
    log_sum, corrected, key_terms, scores = block_terms(
        query, keys, values, strength_blocks, decay_blocks
    )

    def advance(memory, inputs):
        query_block, keys_block, corrected_block, terms_block, scores_block, log_block = inputs
        extended = jnp.concatenate([jnp.zeros_like(corrected_block), corrected_block], axis=-1)
        fresh = extended - jnp.einsum("hcd,hde->hce", terms_block, memory, precision=HIGHEST)
        output = jnp.einsum(
            "hcd,hde->hce", query_block * jnp.exp(log_block)[..., None], memory, precision=HIGHEST
        )
        output = output + jnp.einsum("hcs,hse->hce", scores_block, fresh, precision=HIGHEST)
        tail_log = log_block[:, -1:]
        weighted = keys_block * jnp.exp(tail_log - log_block)[..., None]
        memory = memory * jnp.exp(tail_log)[..., None] + jnp.einsum(
            "hcd,hce->hde", weighted, fresh, precision=HIGHEST
        )
        return (memory, output)

    start_state = jnp.concatenate(
        [
            jnp.broadcast_to(
                jnp.eye(head_size, dtype=jnp.float32), (heads_here, head_size, head_size)
            ),
            jnp.zeros((heads_here, head_size, head_size), jnp.float32),
        ],
        axis=-1,
    )
    sequence_inputs = tuple(
        (jnp.moveaxis(item, 1, 0) for item in (query, keys, corrected, key_terms, scores, log_sum))
    )
    final, outputs = lax.scan(advance, start_state, sequence_inputs)
    outputs = jnp.moveaxis(outputs, 0, 1).reshape(heads_here, rows_here, 2 * head_size)

    def compose(earlier, later):
        moved = jnp.einsum("hij,hjk->hik", later[..., :head_size], earlier, precision=HIGHEST)
        return moved + jnp.concatenate(
            [jnp.zeros_like(later[..., :head_size]), later[..., head_size:]], axis=-1
        )

    prefix = entering(final, "sp", compose, start_state)
    carried = prefix[..., head_size:]
    result = outputs[..., head_size:] + jnp.einsum(
        "htd,hde->hte", outputs[..., :head_size], carried, precision=HIGHEST
    )
    result = jnp.transpose(result, (1, 0, 2))
    result = (
        result
        * lax.rsqrt(jnp.mean(result * result, axis=-1, keepdims=True) + TINY_NORM)
        * head_gain
    )
    delta_mixed = (
        result.reshape(rows_here, heads_here * head_size)
        * jax.nn.silu(delta_gate_raw.astype(jnp.float32))
    ).astype(jnp.bfloat16)
    kernel = conv_taps.shape[0]
    channels = conv_taps.shape[1]
    gated_units = (
        glu_value_raw.astype(jnp.float32) * jax.nn.sigmoid(glu_gate_raw.astype(jnp.float32))
    ).astype(jnp.bfloat16)
    before = shifted(gated_units[rows_here - (kernel - 1) :], "sp", 1)
    padded = jnp.concatenate([before, gated_units], axis=0)
    filtered = jnp.zeros((rows_here, channels), jnp.float32)
    for offset in range(kernel):
        filtered = filtered + padded[offset : offset + rows_here].astype(jnp.float32) * conv_taps[
            offset
        ].astype(jnp.float32)
    first_sum = jnp.sum(filtered, axis=1)
    second_sum = jnp.sum(filtered * filtered, axis=1)
    first_sum, second_sum = lax.psum((first_sum, second_sum), "tp")
    channels_all = channels * tp_size
    center = first_sum / channels_all
    variance = jnp.maximum(second_sum / channels_all - center * center, 0.0)
    normed = (filtered - center[:, None]) * lax.rsqrt(variance + TINY_VAR)[
        :, None
    ] * ln_gain + ln_shift
    conv_mixed = (jax.nn.silu(normed) * jax.nn.silu(conv_gate_raw.astype(jnp.float32))).astype(
        jnp.bfloat16
    )
    summed = jnp.dot(delta_mixed, out_delta, preferred_element_type=jnp.float32)
    return lax.psum_scatter(
        (summed + jnp.dot(conv_mixed, out_conv, preferred_element_type=jnp.float32)).astype(
            jnp.bfloat16
        ),
        "tp",
        scatter_dimension=0,
        tiled=True,
    )


def solution(mesh):
    return jax.shard_map(
        local,
        mesh=mesh,
        in_specs=(
            P("sp", "tp"),
            P(None, "tp"),
            P(None, "tp"),
            P(None, "tp"),
            P(None, "tp"),
            P(None, "tp"),
            P(None, "tp"),
            P(None, "tp"),
            P(),
            P(),
            P(),
            P(),
            P(None, "tp"),
            P("tp"),
            P("tp"),
            P("tp", None),
            P("tp", None),
        ),
        out_specs=P(("sp", "tp"), None),
        check_vma=False,
    )
```

profile of v0, /device:TPU:0, one launch (start us, length us, event | category | flops | bytes accessed | tf_op | source)
XLA Modules:
  0.0 483.8 jit_solution(3299517887842109902)
XLA Ops:
  9.5 36.6 %all-gather.4.cloned.1.call-done = bf16[1024,2048]{1,0:T(8,128)(2,1)} async-done(((bf16[1024,512]{1,0:T(8,128)(2,1)}), bf16[1024,2048]{1,0:T(8,128)(2,1)}) %all-gather.4.cloned.1.call-update) | async-done | bytes 4194320 | tf_op jit(solution)/shard_map/all_gather | solution.py:87
  46.1 3.2 multiply_reduce_fusion
  52.8 3.4 fusion.45
  56.2 1.5 reshape.152
  57.8 3.7 fusion.47
  62.4 4.7 fusion.43
  67.2 1.7 reshape.118
  69.9 3.8 fusion.39
  73.7 158.7 %custom-call.4 = f32[2,16,1,64,64]{3,4,2,1,0:T(8,128)} custom-call(f32[2,16,1,64,64]{4,3,2,1,0:T(8,128)} %fusion.39), custom_call_target="InvertDiagBlocksLowerTriangular" | custom-call | tf_op jit(solution)/shard_map/jit(_solve_triangular)/vmap(vmap())/triangular_solve | solution.py:46
  232.4 2.1 bitcast_multiply_fusion.7
  234.5 2.0 fusion.16
  236.5 1.6 slice_bitcast_fusion
  240.8 3.1 fusion.26
  243.9 104.2 %while.22 = (s32[]{:T(128)}, f32[2,128,256]{2,1,0:T(8,128)S(1)}, f32[16,2,64,256]{3,2,1,0:T(8,128)}, f32[16,2,64]{2,0,1:T(8,128)S(1)}, f32[16,2,64,128]{3,2,1,0:...) while((s32[]{:T(128)}, f32[2,128,256]{2,1,0:T(8,128)S(1)}, ...), condition=%wide.region_5.6_spmd, body=%wide.region_4.5_spmd.sunk | while | flops 176390272 | bytes 2298537 | solution.py:150
  247.4 1.3 convolution_add_fusion.6
  248.7 1.8 fusion.190
  253.9 1.3 convolution_add_fusion.6
  255.2 1.7 fusion.190
  260.4 1.3 convolution_add_fusion.6
  261.7 1.8 fusion.190
  268.3 1.8 fusion.190
  274.8 1.8 fusion.190
  279.9 1.3 convolution_add_fusion.6
  281.3 1.8 fusion.190
  286.5 1.3 convolution_add_fusion.6
  287.8 1.7 fusion.190
  293.0 1.3 convolution_add_fusion.6
  294.3 1.8 fusion.190
  300.8 1.8 fusion.190
  307.3 1.7 fusion.190
  313.8 1.8 fusion.190
  320.4 1.7 fusion.190
  325.5 1.3 convolution_add_fusion.6
  326.9 1.8 fusion.190
  333.4 1.8 fusion.190
  339.9 1.7 fusion.190
  345.0 1.3 convolution_add_fusion.6
  346.4 1.8 fusion.190
  349.0 3.6 fusion.58
  354.8 3.5 collective-permute-start
  358.9 1.8 copy.62
  360.8 6.0 %fusion.142 = (f32[1024]{0:T(1024)S(1)}, f32[1024]{0:T(1024)S(1)}, f32[1024,256]{1,0:T(8,128)}) fusion(f32[256]{0:T(256)S(1)} %bitcast.215, bf16[1024,256]{1,0:T(8,128)(2,1)S(1)} %copy-done.10, f32[256]{0:T(256)S(1)} %bitcast.216, bf16[30,256]{1,0:T(8,128)(2,1)S(1)} %collective-permute-done, f32[256]{0:T(256)S(1)} %bitcast.187, f32[256]{0:T(256)S(1)} %bitcast.188, ...), kind=kLoop, calls=%fused_computation.252 | loop fusion | flops 48494592 | bytes 1628160 | tf_op jit(solution)/shard_map/reduce_sum | solution.py:186
  366.8 6.3 %all-reduce.3 = (f32[1024]{0:T(1024)S(1)}, f32[1024]{0:T(1024)S(1)}) all-reduce(f32[1024]{0:T(1024)S(1)} %get-tuple-element.109, f32[1024]{0:T(1024)S(1)} %get-tuple-element.108), channel_id=1, replica_groups=mesh['sp'=8,'tp'=4] {'tp'}, use_global_device_ids=true, to_apply=%region_12.13 | all-reduce | flops 2048 | bytes 16384 | tf_op jit(solution)/shard_map/psum | solution.py:188
  373.1 25.1 %all-gather.6.cloned.1.call-done = f32[16,128,256]{2,1,0:T(8,128)} async-done(((f32[2,128,256]{2,1,0:T(8,128)}), f32[16,128,256]{2,1,0:T(8,128)}) %all-gather.6.cloned.1.call-update) | async-done | bytes 2097168 | tf_op jit(solution)/shard_map/all_gather | solution.py:16
  399.0 2.9 multiply_reduce_fusion.2
  402.0 10.6 %fusion.65 = f32[1024,2048]{1,0:T(8,128)} fusion(bf16[256,2048]{1,0:T(8,128)(2,1)S(1)} %copy-done, bf16[1024,2048]{1,0:T(8,128)(2,1)} %all-gather.4.cloned.1.call-done, bf16[2048,256]{1,0:T(8,128)(2,1)} %param.25, f32[1024]{0:T(1024)S(1)} %add_rsqrt_fusion.4, f32[1024,2,128]{2,0,1:T(8,128)} %get-tuple-element.185, f32[128]{0:T(128)S(1)} %copy-done.22, ...), kind=kOutput, calls=%fused_computation.110 | convolution fusion | flops 2150367232 | bytes 15741440 | tf_op jit(solution)/shard_map/dot_general | solution.py:198
  412.6 11.5 %add_convert_fusion = bf16[1024,2048]{1,0:T(8,128)(2,1)} fusion(f32[1024,2048]{1,0:T(8,128)} %fusion.65, bf16[256,2048]{1,0:T(8,128)(2,1)S(1)} %copy-done.26, bf16[1024,2048]{1,0:T(8,128)(2,1)} %all-gather.4.cloned.1.call-done, bf16[2048,256]{1,0:T(8,128)(2,1)} %param.28, f32[1024,256]{1,0:T(8,128)S(1)} %copy-done.8, f32[256]{0:T(256)S(1)} %copy-done.27, ...), kind=kOutput, calls=%fused_computation.28 | convolution fusion | flops 2156134400 | bytes 19937280 | tf_op jit(solution)/shard_map/dot_general | solution.py:200
  424.2 53.2 %reduce-scatter.2.cloned.1.call-done = bf16[256,2048]{1,0:T(8,128)(2,1)} async-done(((bf16[1024,2048]{1,0:T(8,128)(2,1)}), bf16[256,2048]{1,0:T(8,128)(2,1)}) %reduce-scatter.2.cloned.1.call-update) | async-done | bytes 1048592 | tf_op jit(solution)/shard_map/reduce_scatter | solution.py:199
  (202 shorter events, 80.2 us)
Async XLA Ops:
  6.5 395.4 %copy-start = (bf16[256,2048]{1,0:T(8,128)(2,1)S(1)}, bf16[256,2048]{1,0:T(8,128)(2,1)}, u32[]{:S(2)}) copy-start(bf16[256,2048]{1,0:T(8,128)(2,1)} %param.36) | copy-start | bytes 3145732
  6.5 42.8 %copy-start.13 = (bf16[2048,8]{0,1:T(8,128)(2,1)S(1)}, bf16[2048,8]{0,1:T(8,128)(2,1)}, u32[]{:S(2)}) copy-start(bf16[2048,8]{0,1:T(8,128)(2,1)} %param.29) | copy-start | bytes 98308
  6.5 39.6 %all-gather.4.cloned.1.call-start = ((), (), s32[]{:S(2)}) async-start(), calls=%async_computation.1 | async-start | bytes 5242880 | tf_op jit(solution)/shard_map/all_gather | solution.py:87
  7.3 390.9 %all-gather.6.cloned.1.call-start = ((), (), s32[]{:S(2)}) async-start(), calls=%async_computation.3 | async-start | bytes 2359296 | tf_op jit(solution)/shard_map/all_gather | solution.py:16
  7.4 50.4 %copy-start.3 = (f32[2,128,256]{2,1,0:T(8,128)}, f32[2,128,256]{2,1,0:T(8,128)S(1)}, u32[]{:S(2)}) copy-start(f32[2,128,256]{2,1,0:T(8,128)S(1)} %concatenate.15) | copy-start | bytes 786436
  46.1 3.4 copy-start.1
  46.1 4.6 copy-start.14
  49.6 3.2 copy-start.23
  62.4 7.5 %copy-start.12 = (f32[64,64]{1,0:T(8,128)S(1)}, f32[64,64]{1,0:T(8,128)}, u32[]{:S(2)}) copy-start(f32[64,64]{1,0:T(8,128)} %get-tuple-element.189) | copy-start | bytes 49156
  62.4 7.5 %copy-start.16 = (pred[64,64]{1,0:T(8,128)(4,1)S(1)}, pred[64,64]{1,0:T(8,128)(4,1)}, u32[]{:S(2)}) copy-start(pred[64,64]{1,0:T(8,128)(4,1)} %get-tuple-element.187) | copy-start | bytes 12292
  62.4 7.5 %copy-start.17 = (pred[64,64]{1,0:T(8,128)(4,1)S(1)}, pred[64,64]{1,0:T(8,128)(4,1)}, u32[]{:S(2)}) copy-start(pred[64,64]{1,0:T(8,128)(4,1)} %get-tuple-element.188) | copy-start | bytes 12292
  232.4 2.1 copy-start.7
  236.5 4.3 copy-start.15
  238.1 5.8 %copy-start.6 = (f32[2,128,256]{2,1,0:T(8,128)S(1)}, f32[2,128,256]{2,1,0:T(8,128)}, u32[]{:S(2)}) copy-start(f32[2,128,256]{2,1,0:T(8,128)} %copy-done.3) | copy-start | bytes 786436
  243.9 105.0 %copy-start.11 = (bf16[31,256]{1,0:T(8,128)(2,1)S(1)}, bf16[31,256]{1,0:T(8,128)(2,1)}, u32[]{:S(2)}) copy-start(bf16[31,256]{1,0:T(8,128)(2,1)} %param.33) | copy-start | bytes 47620
  243.9 105.1 %copy-start.24 = (bf16[2048,256]{1,0:T(8,128)(2,1)S(1)}, bf16[2048,256]{1,0:T(8,128)(2,1)}, u32[]{:S(2)}) copy-start(bf16[2048,256]{1,0:T(8,128)(2,1)} %param.27) | copy-start | bytes 3145732
  348.1 0.7 copy-start.5
  348.9 128.4 %reduce-scatter.2.cloned.1.call-start = ((), (), s32[]{:S(2)}) async-start(), calls=%async_computation.2 | async-start | bytes 5242880 | tf_op jit(solution)/shard_map/reduce_scatter | solution.py:199
  349.0 3.7 copy-start.2
  349.0 3.7 copy-start.25
  354.0 0.8 copy-start.9
  354.8 43.4 %copy-start.4 = (f32[2,128,256]{2,1,0:T(8,128)S(1)}, f32[2,128,256]{2,1,0:T(8,128)}, u32[]{:S(2)}) copy-start(f32[2,128,256]{2,1,0:T(8,128)} %copy-done.3) | copy-start | bytes 786436
  354.8 5.9 %collective-permute-start = (bf16[30,256]{1,0:T(8,128)(2,1)S(1)}, bf16[30,256]{1,0:T(8,128)(2,1)S(1)}, u32[]{:S(2)}, u32[]{:S(2)}) collective-permute-start(bf16[30,256]{1,0:T(8,128)(2,1)S(1)} %slice.292), channel_id=1, source_target_pairs={{0,4},{4,8},{8,12},{12,16},{16,20},{20,24},{24,28},{1,5},{5,9},{9,... | collective-permute-start | bytes 46088 | tf_op jit(solution)/shard_map/ppermute | solution.py:28
  358.9 1.9 copy-start.10
  358.9 1.9 copy-start.18
  358.9 1.9 copy-start.19
  358.9 1.9 copy-start.20
  358.9 1.9 copy-start.21
  398.2 3.8 copy-start.22
  401.9 10.6 %copy-start.8 = (f32[1024,256]{1,0:T(8,128)S(1)}, f32[1024,256]{1,0:T(8,128)}, u32[]{:S(2)}) copy-start(f32[1024,256]{1,0:T(8,128)} %get-tuple-element.138) | copy-start | bytes 3145732
  402.0 10.6 %copy-start.26 = (bf16[256,2048]{1,0:T(8,128)(2,1)S(1)}, bf16[256,2048]{1,0:T(8,128)(2,1)}, u32[]{:S(2)}) copy-start(bf16[256,2048]{1,0:T(8,128)(2,1)} %param.37) | copy-start | bytes 3145732
  402.0 10.6 %copy-start.27 = (f32[256]{0:T(256)S(1)}, f32[256]{0:T(256)}, u32[]{:S(2)}) copy-start(f32[256]{0:T(256)} %param.35) | copy-start | bytes 3076
  402.0 10.6 %copy-start.28 = (f32[256]{0:T(256)S(1)}, f32[256]{0:T(256)}, u32[]{:S(2)}) copy-start(f32[256]{0:T(256)} %param.34) | copy-start | bytes 3076
Sparse Core Ops, SparseCore 0:
  8.9 37.1 all-gather.3
  349.0 49.1 all-gather.5
  424.3 52.9 reduce-scatter.1
where the time goes:
time: 488 us; the launch traced here: 484 us
  other arithmetic  178 us (36%)
  matrix products  139 us (28%)
  waiting for transfers between devices  116 us (24%)
  local copies, waits for them, and re-layouts  27.1 us (6%)
  between operations  13.6 us (3%)
  blocking collectives  6.3 us (1%)
    another operation x4, other arithmetic, block_terms(): jax.scipy.linalg.solve_triangular(identity + lower, right, lower=True, un...  159 us
    reduce_scatter x1, waiting for transfers between devices, local(): lax.psum_scatter((summed + jnp.dot(conv_mixed, out_conv, preferred_elemen...  53.2 us
    all_gather x1, waiting for transfers between devices, local(): piece = lax.all_gather(tokens, 'tp', axis=1, tiled=True)  36.6 us
    dot_general x16, matrix products, advance(): jnp.einsum('hcs,hse->hce', scores_block, fresh, precision=HIGHEST)  28.1 us
    all_gather x1, waiting for transfers between devices, entering(): gathered = lax.all_gather(part, axis)  25.1 us
    dot_general x16, matrix products, advance(): jnp.einsum('hcd,hce->hde', weighted, fresh, precision=HIGHEST)  21.5 us
    dot_general x7, matrix products, local(): jnp.dot(piece, weight, preferred_element_type=jnp.float32)  19.2 us
    dot_general x16, matrix products, advance(): jnp.einsum('hcd,hde->hce', query_block * jnp.exp(log_block)[..., None], m...  18.5 us
  transfers between devices with their start and end apart: 4, of which 3 were waited for; matrix products, arithmetic and copies ran while one was open for 3% of the time, Pallas kernels for 0%

commit v1 on v0

v1 whole, which is shorter than its diff:
```python
import functools

import jax
import jax.numpy as jnp
from jax import lax
from jax.experimental import pallas as pl
from jax.experimental.pallas import tpu as pltpu
from jax.sharding import PartitionSpec as P

BLOCK = 128


TINY_NORM = 1e-06
TINY_VAR = 1e-05
HIGHEST = lax.Precision.HIGHEST


def shifted(block, axis, distance):
    devices = range(lax.axis_size(axis))
    route = [(i - distance, i) for i in devices if i - distance in devices]
    return lax.ppermute(block, axis, route)


def nt(a, b):
    return lax.dot_general(a, b, (((1,), (1,)), ((), ())), preferred_element_type=jnp.float32)


def mm(a, b):
    return jnp.dot(
        a.astype(jnp.bfloat16), b.astype(jnp.bfloat16), preferred_element_type=jnp.float32
    )


def delta_kernel(
    heads, width, q_ref, k_ref, v_ref, g_ref, outa_ref, outb_ref, state_ref,
    lhs_s, corr_s, score_s, wt_s, tail_s,
):
    rows = q_ref.shape[0]
    blocks = rows // BLOCK
    row_id = lax.broadcasted_iota(jnp.int32, (BLOCK, BLOCK), 0)
    col_id = lax.broadcasted_iota(jnp.int32, (BLOCK, BLOCK), 1)
    causal = row_id >= col_id
    strict = row_id > col_id
    differ = row_id ^ col_id
    eye = jnp.where(row_id == col_id, 1.0, 0.0)
    tril = jnp.where(causal, 1.0, 0.0)

    def prepare(c):
        at = pl.ds(pl.multiple_of(c * BLOCK, BLOCK), BLOCK)
        gates = g_ref[at, :]
        sums = jnp.dot(tril, gates, precision=HIGHEST, preferred_element_type=jnp.float32)
        chains = []
        for h in range(heads):
            lanes = slice(h * width, (h + 1) * width)
            k, q = k_ref[at, lanes], q_ref[at, lanes]
            v = v_ref[at, lanes].astype(jnp.float32)
            kf, qf = k.astype(jnp.float32), q.astype(jnp.float32)
            ik = lax.rsqrt(jnp.sum(kf * kf, axis=-1, keepdims=True) + TINY_NORM)
            iq = lax.rsqrt(jnp.sum(qf * qf, axis=-1, keepdims=True) + TINY_NORM)
            iq = iq * width ** (-0.5)
            beta = gates[:, h : h + 1]
            log_sum = sums[:, heads + h : heads + h + 1]
            log_full = jnp.broadcast_to(log_sum, (BLOCK, BLOCK))
            spread = log_full - log_full.T
            damp = jnp.where(causal, jnp.exp(jnp.where(causal, spread, 0.0)), 0.0)
            damp = damp * jnp.broadcast_to(ik, (BLOCK, BLOCK)).T
            lower = jnp.where(strict, nt(k, k) * damp * (beta * ik), 0.0)
            score_s[h, at, :] = (nt(q, k) * damp * iq).astype(jnp.bfloat16)
            grow = jnp.exp(log_sum)
            right = jnp.concatenate([v * beta, kf * (beta * ik * grow)], axis=1)
            tail = log_full[BLOCK - 1 : BLOCK, :]
            weighted = kf * (ik * jnp.exp(tail[:, :1] - log_sum))
            wt_s[h, c] = weighted.T.astype(jnp.bfloat16)
            tail_s[h, c] = jnp.broadcast_to(jnp.exp(tail), (8, BLOCK))
            lhs_s[h, c, BLOCK:, :] = (qf * (iq * grow)).astype(jnp.bfloat16)
            chains.append([h, lower, right, eye - jnp.where(differ == 1, lower, 0.0)])
        return at, c, chains

    def pair(p, carry):
        prepared = [prepare(p * 2 + i) for i in range(2)]
        size = 2
        while size < BLOCK:
            level = (differ >= size) & (differ < 2 * size)
            parts = [
                [mm(jnp.where(level, ch[1], 0.0), ch[3]) for ch in item[2]] for item in prepared
            ]
            for item, part in zip(prepared, parts):
                for ch, moved in zip(item[2], part):
                    ch[3] = ch[3] - mm(ch[3], moved)
            size *= 2
        for at, c, chains in prepared:
            for h, lower, right, inverse in chains:
                solved = mm(inverse, right)
                corr_s[h, at, :] = solved[:, :width]
                lhs_s[h, c, :BLOCK, :] = solved[:, width:].astype(jnp.bfloat16)
        return carry

    lax.fori_loop(0, blocks // 2, pair, 0)
    for h in range(heads):
        state_ref[h] = jnp.concatenate([eye, jnp.zeros((width, width), jnp.float32)], axis=1)

    def advance(c, carry):
        at = pl.ds(pl.multiple_of(c * BLOCK, BLOCK), BLOCK)
        boths = [mm(lhs_s[h, c], state_ref[h]) for h in range(heads)]
        fresh = []
        for h in range(heads):
            first = boths[h][:BLOCK]
            fresh.append(
                jnp.concatenate(
                    [-first[:, :width], corr_s[h, at, :] - first[:, width:]], axis=1
                ).astype(jnp.bfloat16)
            )
        for h in range(heads):
            decay = tail_s[h, c][:1, :]
            decay = jnp.concatenate([decay, decay], axis=1)
            state_ref[h] = state_ref[h] * decay + mm(wt_s[h, c], fresh[h])
        for h in range(heads):
            out = boths[h][BLOCK:] + mm(score_s[h, at, :], fresh[h])
            outa_ref[h, at, :] = out[:, :width].astype(jnp.bfloat16)
            outb_ref[h, at, :] = out[:, width:]
        return carry

    lax.fori_loop(0, blocks, advance, 0)


def delta_rule(query_raw, key_raw, value_raw, gates, heads, width):
    rows = query_raw.shape[0]
    blocks = rows // BLOCK
    vm = pl.BlockSpec(memory_space=pltpu.VMEM)
    return pl.pallas_call(
        functools.partial(delta_kernel, heads, width),
        out_shape=(
            jax.ShapeDtypeStruct((heads, rows, width), jnp.bfloat16),
            jax.ShapeDtypeStruct((heads, rows, width), jnp.float32),
            jax.ShapeDtypeStruct((heads, width, 2 * width), jnp.float32),
        ),
        in_specs=[vm] * 4,
        out_specs=(vm, vm, vm),
        scratch_shapes=[
            pltpu.VMEM((heads, blocks, 2 * BLOCK, width), jnp.bfloat16),
            pltpu.VMEM((heads, rows, width), jnp.float32),
            pltpu.VMEM((heads, rows, BLOCK), jnp.bfloat16),
            pltpu.VMEM((heads, blocks, width, BLOCK), jnp.bfloat16),
            pltpu.VMEM((heads, blocks, 8, BLOCK), jnp.float32),
        ],
        compiler_params=pltpu.CompilerParams(
            vmem_limit_bytes=40 * 1024 * 1024
        ),
        cost_estimate=pl.CostEstimate(
            flops=10_000_000_000, bytes_accessed=4_000_000, transcendentals=0
        ),
        name="delta_rule",
    )(query_raw, key_raw, value_raw, gates)


def finish_kernel(
    heads, width, place_ref, all_ref, outa_ref, outb_ref, gate_ref, gain_ref, mixed_ref, carry_s
):
    rows = outb_ref.shape[1]
    carry_s[...] = jnp.zeros_like(carry_s)

    def hop(i, carry):
        moved = [
            jnp.dot(
                all_ref[i, h, :, :width],
                carry_s[h],
                precision=HIGHEST,
                preferred_element_type=jnp.float32,
            )
            for h in range(heads)
        ]
        for h in range(heads):
            carry_s[h] = moved[h] + all_ref[i, h, :, width:]
        return carry

    lax.fori_loop(0, place_ref[0], hop, 0)
    tile = 256

    def one(c, carry):
        at = pl.ds(pl.multiple_of(c * tile, tile), tile)
        for h in range(heads):
            lanes = slice(h * width, (h + 1) * width)
            result = outb_ref[h, at, :] + mm(outa_ref[h, at, :], carry_s[h])
            result = result * lax.rsqrt(
                jnp.mean(result * result, axis=-1, keepdims=True) + TINY_NORM
            )
            gate = gate_ref[at, lanes].astype(jnp.float32)
            mixed_ref[at, lanes] = (result * gain_ref[...] * jax.nn.silu(gate)).astype(
                jnp.bfloat16
            )
        return carry

    lax.fori_loop(0, rows // tile, one, 0)


def finish(place, states, outa, outb, gate, gain, heads, width):
    rows = outb.shape[1]
    vm = pl.BlockSpec(memory_space=pltpu.VMEM)
    return pl.pallas_call(
        functools.partial(finish_kernel, heads, width),
        out_shape=jax.ShapeDtypeStruct((rows, heads * width), jnp.bfloat16),
        in_specs=[pl.BlockSpec(memory_space=pltpu.SMEM)] + [vm] * 5,
        out_specs=vm,
        scratch_shapes=[pltpu.VMEM((heads, width, width), jnp.float32)],
        compiler_params=pltpu.CompilerParams(vmem_limit_bytes=40 * 1024 * 1024),
        cost_estimate=pl.CostEstimate(
            flops=2_000_000_000, bytes_accessed=6_000_000, transcendentals=0
        ),
        name="delta_finish",
    )(place, states, outa, outb, gate, gain)


def local(
    tokens,
    w_query,
    w_key,
    w_value,
    w_delta_gate,
    w_glu_value,
    w_glu_gate,
    w_conv_gate,
    w_beta,
    w_decay,
    decay_log,
    head_gain,
    conv_taps,
    ln_gain,
    ln_shift,
    out_delta,
    out_conv,
):
    rows_here = tokens.shape[0]
    tp_size = lax.axis_size("tp")
    width_all = tokens.shape[1] * tp_size
    weights = (
        w_query,
        w_key,
        w_value,
        w_delta_gate,
        w_glu_value,
        w_glu_gate,
        w_conv_gate,
        w_beta,
        w_decay,
    )
    piece = lax.all_gather(tokens, "tp", axis=1, tiled=True)
    totals = tuple(
        (jnp.dot(piece, weight, preferred_element_type=jnp.float32) for weight in weights)
    )
    squares = jnp.sum(jnp.square(piece.astype(jnp.float32)), axis=1)
    sums, squares = (totals, squares)
    inv_rms = lax.rsqrt(squares / width_all + TINY_NORM)[:, None]
    scaled = [summed * inv_rms for summed in sums]
    query_raw, key_raw, value_raw, delta_gate_raw, glu_value_raw, glu_gate_raw, conv_gate_raw = [
        item.astype(jnp.bfloat16) for item in scaled[:7]
    ]
    head_size = head_gain.shape[0]
    heads_here = w_query.shape[1] // head_size
    first_head = lax.axis_index("tp") * heads_here
    strength = jax.nn.sigmoid(lax.dynamic_slice_in_dim(scaled[7], first_head, heads_here, 1))
    rates = jnp.exp(lax.dynamic_slice_in_dim(decay_log, first_head, heads_here, 0))
    log_decay = -rates[None, :] * jax.nn.softplus(
        lax.dynamic_slice_in_dim(scaled[8], first_head, heads_here, 1)
    )
    gates = jnp.concatenate(
        [
            strength,
            log_decay,
            jnp.zeros((rows_here, head_size - 2 * heads_here), jnp.float32),
        ],
        axis=1,
    )
    outa, outb, final = delta_rule(
        query_raw, key_raw, value_raw, gates, heads_here, head_size
    )
    states = lax.all_gather(final, "sp")
    place = lax.axis_index("sp").astype(jnp.int32).reshape(1)
    delta_mixed = finish(
        place, states, outa, outb, delta_gate_raw, head_gain[None, :], heads_here, head_size
    )
    kernel = conv_taps.shape[0]
    channels = conv_taps.shape[1]
    gated_units = (
        glu_value_raw.astype(jnp.float32) * jax.nn.sigmoid(glu_gate_raw.astype(jnp.float32))
    ).astype(jnp.bfloat16)
    before = shifted(gated_units[rows_here - (kernel - 1) :], "sp", 1)
    padded = jnp.concatenate([before, gated_units], axis=0)
    filtered = jnp.zeros((rows_here, channels), jnp.float32)
    for offset in range(kernel):
        filtered = filtered + padded[offset : offset + rows_here].astype(jnp.float32) * conv_taps[
            offset
        ].astype(jnp.float32)
    first_sum = jnp.sum(filtered, axis=1)
    second_sum = jnp.sum(filtered * filtered, axis=1)
    first_sum, second_sum = lax.psum((first_sum, second_sum), "tp")
    channels_all = channels * tp_size
    center = first_sum / channels_all
    variance = jnp.maximum(second_sum / channels_all - center * center, 0.0)
    normed = (filtered - center[:, None]) * lax.rsqrt(variance + TINY_VAR)[
        :, None
    ] * ln_gain + ln_shift
    conv_mixed = (jax.nn.silu(normed) * jax.nn.silu(conv_gate_raw.astype(jnp.float32))).astype(
        jnp.bfloat16
    )
    summed = jnp.dot(delta_mixed, out_delta, preferred_element_type=jnp.float32)
    return lax.psum_scatter(
        (summed + jnp.dot(conv_mixed, out_conv, preferred_element_type=jnp.float32)).astype(
            jnp.bfloat16
        ),
        "tp",
        scatter_dimension=0,
        tiled=True,
    )


def solution(mesh):
    return jax.shard_map(
        local,
        mesh=mesh,
        in_specs=(
            P("sp", "tp"),
            P(None, "tp"),
            P(None, "tp"),
            P(None, "tp"),
            P(None, "tp"),
            P(None, "tp"),
            P(None, "tp"),
            P(None, "tp"),
            P(),
            P(),
            P(),
            P(),
            P(None, "tp"),
            P("tp"),
            P("tp"),
            P("tp", None),
            P("tp", None),
        ),
        out_specs=P(("sp", "tp"), None),
        check_vma=False,
    )
```

time: 488 us -> 191 us (0.39)
  other arithmetic: 178 us -> 10.6 us
  matrix products: 139 us -> 28.7 us
  local copies, waits for them, and re-layouts: 27.1 us -> 2.05 us
  Pallas kernels: 0 us -> 15.9 us
  waiting for transfers between devices: 116 us -> 111 us
    another operation x5 -> x0, other arithmetic: 160 us -> none  [the longest x4 159 us: block_terms(): jax.scipy.linalg.solve_triangular(identity + lower, right, lower=True, un...]
    dot_general x67 -> x0, matrix products: 95.6 us -> none  [the longest x16 28.1 us: advance(): jnp.einsum('hcs,hse->hce', scores_block, fresh, precision=HIGHEST)]
    pallas_call x0 -> x2, Pallas kernels: none -> 15.9 us  [the longest x1 14.6 us: delta_rule(): pl.pallas_call(functools.partial(delta_kernel, heads, width), out_shape=(...]
    squeeze x16 -> x0, local copies, waits for them, and re-layouts: 13.8 us -> none  [local(): final, outputs = lax.scan(advance, start_state, sequence_inputs)]
    reduce_scatter x1, waiting for transfers between devices: 53.2 us -> 45.1 us  [local(): lax.psum_scatter((summed + jnp.dot(conv_mixed, out_conv, preferred_elemen...]
    dot_general x7 -> x8, matrix products: 19.2 us -> 12.6 us  [local(): jnp.dot(piece, weight, preferred_element_type=jnp.float32)]
    dot_general x1, matrix products: 10.6 us -> 4.5 us  [local(): summed = jnp.dot(delta_mixed, out_delta, preferred_element_type=jnp.float32)]
    transpose x3 -> x0, local copies, waits for them, and re-layouts: 4.94 us -> none  [the longest x1 1.81 us: local(): jnp.moveaxis(outputs, 0, 1).reshape(heads_here, rows_here, 2 * head_size)]
  transfers between devices with their start and end apart: 4 -> 4, of which waited for: 3 -> 4; matrix products, arithmetic and copies ran while one was open for 3% -> 7% of each run, Pallas kernels for 0% -> 0%
where the time goes in v1:
time: 191 us
  waiting for transfers between devices  111 us (58%)
  matrix products  28.7 us (15%)
  Pallas kernels  15.9 us (8%)
  between operations  13.4 us (7%)
  other arithmetic  10.6 us (6%)
  blocking collectives  6.23 us (3%)
  starting transfers between devices  3.64 us (2%)
  local copies, waits for them, and re-layouts  2.05 us (1%)
    reduce_scatter x1, waiting for transfers between devices, local(): lax.psum_scatter((summed + jnp.dot(conv_mixed, out_conv, preferred_elemen...  45.1 us
    all_gather x1, waiting for transfers between devices, local(): piece = lax.all_gather(tokens, 'tp', axis=1, tiled=True)  38 us
    all_gather x1, waiting for transfers between devices, local(): states = lax.all_gather(final, 'sp')  26.6 us
    pallas_call x1, Pallas kernels, delta_rule(): pl.pallas_call(functools.partial(delta_kernel, heads, width), out_shape=(...  14.6 us
    dot_general x8, matrix products, local(): jnp.dot(piece, weight, preferred_element_type=jnp.float32)  12.6 us
    dot_general x1, matrix products, local(): jnp.dot(conv_mixed, out_conv, preferred_element_type=jnp.float32)  11.5 us
    psum x1, blocking collectives, local(): first_sum, second_sum = lax.psum((first_sum, second_sum), 'tp')  6.23 us
    reduce_sum x1, other arithmetic, local(): first_sum = jnp.sum(filtered, axis=1)  5.87 us
  transfers between devices with their start and end apart: 4, of which 4 were waited for; matrix products, arithmetic and copies ran while one was open for 7% of the time, Pallas kernels for 0%

profile of v1, /device:TPU:0, one launch (start us, length us, event | category | flops | bytes accessed | tf_op | source)
XLA Modules:
  0.0 190.9 jit_solution(7346788846913048323)
XLA Ops:
  6.5 0.0 copy-start
  6.5 0.0 all-gather.4.cloned.1.call-start
  6.5 0.7 all-gather.4.cloned.1.call-update
  7.3 0.0 all-gather.6.cloned.1.call-start
  7.3 0.1 pad.4.clone
  7.4 0.7 exponential_negate_fusion
  8.1 38.0 %all-gather.4.cloned.1.call-done = bf16[1024,2048]{1,0:T(8,128)(2,1)} async-done(((bf16[1024,512]{1,0:T(8,128)(2,1)}), bf16[1024,2048]{1,0:T(8,128)(2,1)}) %all-gather.4.cloned.1.call-update) | async-done | bytes 4194320 | tf_op jit(solution)/shard_map/all_gather | solution.py:246
  46.1 3.2 %multiply_reduce_fusion = f32[1024]{0:T(1024)S(1)} fusion(bf16[1024,2048]{1,0:T(8,128)(2,1)} %all-gather.4.cloned.1.call-done), kind=kLoop, calls=%fused_computation.1 | loop fusion | flops 6290432 | bytes 4198400 | tf_op jit(solution)/shard_map/reduce_sum | solution.py:250
  49.4 0.0 copy-done.13
  49.4 0.2 copy-done.3
  49.6 1.2 fusion.67
  50.8 0.0 copy-done.14
  50.8 0.0 copy-start.7
  50.8 1.2 fusion.66
  52.0 0.5 fusion.57
  52.5 0.2 maximum_maximum_fusion.g_ref
  52.8 0.0 copy-done.7
  52.8 0.0 copy-start.8
  52.8 1.3 fusion.1.k_ref
  54.0 0.0 copy-start.9
  54.1 1.3 fusion.2.v_ref
  55.3 1.3 fusion.q_ref
  56.6 0.0 copy-start.6
  56.6 14.6 %delta_rule.1 = (bf16[2,1024,128]{2,1,0:T(8,128)(2,1)S(1)}, f32[2,1024,128]{2,1,0:T(8,128)S(1)}, f32[2,128,256]{2,1,0:T(8,128)}) custom-call(bf16[1024,256]{1,0:T(8,128)(2,1)S(1)} %fusion.q_ref, bf16[1024,256]{1,0:T(8,128)(2,1)S(1)} %fusion.1.k_ref, bf16[1024,256]{1,0:T(8,128)(2,1)S(1)} %fusion.2.v_ref, f32[1024,128]{1,0:T(8,128)S(1)} %maximum_maximum_fusion.g_ref), custom_call_target="tpu_custom_call" | custom-call | flops 10000000000 | bytes 4000000 | tf_op jit(solution)/shard_map/delta_rule/pallas_call | solution.py:130
  71.2 0.0 all-gather.6.cloned.1.call-update
  71.3 0.0 reduce-scatter.2.cloned.1.call-start
  71.4 0.0 copy-start.4
  71.4 0.0 copy-start.10
  71.4 3.9 %fusion.13 = f32[1024,256]{1,0:T(8,128)S(1)} fusion(bf16[1024,2048]{1,0:T(8,128)(2,1)} %all-gather.4.cloned.1.call-done, bf16[2048,256]{1,0:T(8,128)(2,1)} %param.23, f32[1024]{0:T(1024)S(1)} %add_rsqrt_fusion.1), kind=kOutput, calls=%fused_computation.54 | convolution fusion | flops 1075314688 | bytes 6295552 | tf_op jit(solution)/shard_map/dot_general | solution.py:248
  75.3 0.1 copy-done.10
  75.4 1.3 fusion.7
  76.7 0.0 copy-start.2
  76.7 3.6 %collective-permute-start = (bf16[30,256]{1,0:T(8,128)(2,1)S(1)}, bf16[30,256]{1,0:T(8,128)(2,1)S(1)}, u32[]{:S(2)}, u32[]{:S(2)}) collective-permute-start(bf16[30,256]{1,0:T(8,128)(2,1)S(1)} %slice.248), channel_id=1, source_target_pairs={{0,4},{4,8},{8,12},{12,16},{16,20},{20,24},{24,28},{1,5},{5,9},{9,... | collective-permute-start | bytes 46088 | tf_op jit(solution)/shard_map/ppermute | solution.py:21
  80.3 1.2 fusion.3.gate_ref
  81.5 0.1 collective-permute-done
  81.7 5.9 %fusion.65 = (f32[1024]{0:T(1024)S(1)}, f32[1024]{0:T(1024)S(1)}, f32[1024,256]{1,0:T(8,128)}) fusion(f32[256]{0:T(256)S(1)} %bitcast.67, bf16[1024,256]{1,0:T(8,128)(2,1)S(1)} %fusion.7, f32[256]{0:T(256)S(1)} %bitcast.68, bf16[30,256]{1,0:T(8,128)(2,1)S(1)} %collective-permute-done, f32[256]{0:T(256)S(1)} %bitcast.70, f32[256]{0:T(256)S(1)} %bitcast.71, ...), kind=kLoop, calls=%fused_computation.151 | loop fusion | flops 48494592 | bytes 1628160 | tf_op jit(solution)/shard_map/reduce_sum | solution.py:293
  87.5 6.2 %all-reduce = (f32[1024]{0:T(1024)S(1)}, f32[1024]{0:T(1024)S(1)}) all-reduce(f32[1024]{0:T(1024)S(1)} %get-tuple-element.12, f32[1024]{0:T(1024)S(1)} %get-tuple-element.11), channel_id=1, replica_groups=mesh['sp'=8,'tp'=4] {'tp'}, use_global_device_ids=true, to_apply=%region_4.5 | all-reduce | flops 2048 | bytes 16384 | tf_op jit(solution)/shard_map/psum | solution.py:295
  93.8 26.6 %all-gather.6.cloned.1.call-done = f32[16,128,256]{2,1,0:T(8,128)} async-done(((f32[2,128,256]{2,1,0:T(8,128)}), f32[16,128,256]{2,1,0:T(8,128)}) %all-gather.6.cloned.1.call-update) | async-done | bytes 2097168 | tf_op jit(solution)/shard_map/all_gather | solution.py:276
  120.4 1.6 copy-done.1
  122.0 1.2 delta_finish.1
  123.2 0.0 copy-start.5
  123.2 0.0 copy-start.12
  123.2 0.0 copy-start.15
  123.2 0.0 copy-start.16
  123.2 4.5 %fusion.68 = f32[1024,2048]{1,0:T(8,128)} fusion(bf16[1024,256]{1,0:T(8,128)(2,1)S(1)} %delta_finish.1, bf16[256,2048]{1,0:T(8,128)(2,1)S(1)} %copy-done), kind=kOutput, calls=%fused_computation.154 | convolution fusion | flops 1073741824 | bytes 9961472 | tf_op jit(solution)/shard_map/dot_general | solution.py:305
  127.8 11.5 %add_convert_fusion = bf16[1024,2048]{1,0:T(8,128)(2,1)} fusion(f32[1024,2048]{1,0:T(8,128)} %fusion.68, bf16[256,2048]{1,0:T(8,128)(2,1)S(1)} %copy-done.12, bf16[1024,2048]{1,0:T(8,128)(2,1)} %all-gather.4.cloned.1.call-done, bf16[2048,256]{1,0:T(8,128)(2,1)} %param.24, f32[1024,256]{1,0:T(8,128)S(1)} %copy-done.5, f32[256]{0:T(256)S(1)} %copy-done.15, ...), kind=kOutput, calls=%fused_computation | convolution fusion | flops 2156134400 | bytes 19937280 | tf_op jit(solution)/shard_map/dot_general | solution.py:307
  139.3 0.0 reduce-scatter.2.cloned.1.call-update
  139.3 45.1 %reduce-scatter.2.cloned.1.call-done = bf16[256,2048]{1,0:T(8,128)(2,1)} async-done(((bf16[1024,2048]{1,0:T(8,128)(2,1)}), bf16[256,2048]{1,0:T(8,128)(2,1)}) %reduce-scatter.2.cloned.1.call-update) | async-done | bytes 1048592 | tf_op jit(solution)/shard_map/reduce_scatter | solution.py:306
  (22 shorter events, 0.1 us)
Async XLA Ops:
  6.5 116.7 %copy-start = (bf16[256,2048]{1,0:T(8,128)(2,1)S(1)}, bf16[256,2048]{1,0:T(8,128)(2,1)}, u32[]{:S(2)}) copy-start(bf16[256,2048]{1,0:T(8,128)(2,1)} %param.32) | copy-start | bytes 3145732
  6.5 42.8 %copy-start.13 = (bf16[2048,8]{0,1:T(8,128)(2,1)S(1)}, bf16[2048,8]{0,1:T(8,128)(2,1)}, u32[]{:S(2)}) copy-start(bf16[2048,8]{0,1:T(8,128)(2,1)} %param.26) | copy-start | bytes 98308
  6.5 39.6 %all-gather.4.cloned.1.call-start = ((), (), s32[]{:S(2)}) async-start(), calls=%async_computation.1 | async-start | bytes 5242880 | tf_op jit(solution)/shard_map/all_gather | solution.py:246
  7.3 113.1 %all-gather.6.cloned.1.call-start = ((), (), s32[]{:S(2)}) async-start(), calls=%async_computation.3 | async-start | bytes 2359296 | tf_op jit(solution)/shard_map/all_gather | solution.py:276
  46.1 3.4 %copy-start.3 = (bf16[1024,2048]{1,0:T(8,128)(2,1)S(1)}, bf16[1024,2048]{1,0:T(8,128)(2,1)}, u32[]{:S(2)}) copy-start(bf16[1024,2048]{1,0:T(8,128)(2,1)} %all-gather.4.cloned.1.call-done) | copy-start | bytes 12582916
  46.1 4.7 %copy-start.14 = (bf16[2048,8]{0,1:T(8,128)(2,1)S(1)}, bf16[2048,8]{0,1:T(8,128)(2,1)}, u32[]{:S(2)}) copy-start(bf16[2048,8]{0,1:T(8,128)(2,1)} %param.25) | copy-start | bytes 98308
  50.8 2.0 %copy-start.7 = (bf16[2048,256]{1,0:T(8,128)(2,1)S(1)}, bf16[2048,256]{1,0:T(8,128)(2,1)}, u32[]{:S(2)}) copy-start(bf16[2048,256]{1,0:T(8,128)(2,1)} %param.19) | copy-start | bytes 3145732
  52.8 1.3 copy-start.8
  54.0 1.3 copy-start.9
  56.6 14.7 %copy-start.6 = (bf16[31,256]{1,0:T(8,128)(2,1)S(1)}, bf16[31,256]{1,0:T(8,128)(2,1)}, u32[]{:S(2)}) copy-start(bf16[31,256]{1,0:T(8,128)(2,1)} %param.29) | copy-start | bytes 47620
  71.3 113.2 %reduce-scatter.2.cloned.1.call-start = ((), (), s32[]{:S(2)}) async-start(), calls=%async_computation.2 | async-start | bytes 5242880 | tf_op jit(solution)/shard_map/reduce_scatter | solution.py:306
  71.4 4.0 %copy-start.4 = (bf16[1024,2048]{1,0:T(8,128)(2,1)S(1)}, bf16[1024,2048]{1,0:T(8,128)(2,1)}, u32[]{:S(2)}) copy-start(bf16[1024,2048]{1,0:T(8,128)(2,1)} %all-gather.4.cloned.1.call-done) | copy-start | bytes 12582916
  71.4 4.0 %copy-start.10 = (bf16[2048,256]{1,0:T(8,128)(2,1)S(1)}, bf16[2048,256]{1,0:T(8,128)(2,1)}, u32[]{:S(2)}) copy-start(bf16[2048,256]{1,0:T(8,128)(2,1)} %param.22) | copy-start | bytes 3145732
  75.4 4.9 %copy-start.11 = (bf16[2048,256]{1,0:T(8,128)(2,1)S(1)}, bf16[2048,256]{1,0:T(8,128)(2,1)}, u32[]{:S(2)}) copy-start(bf16[2048,256]{1,0:T(8,128)(2,1)} %param.21) | copy-start | bytes 3145732
  76.7 43.7 %copy-start.2 = (f32[128]{0:T(128)S(1)}, f32[128]{0:T(128)}, u32[]{:S(2)}) copy-start(f32[128]{0:T(128)} %param.28) | copy-start | bytes 1540
  76.7 5.0 %collective-permute-start = (bf16[30,256]{1,0:T(8,128)(2,1)S(1)}, bf16[30,256]{1,0:T(8,128)(2,1)S(1)}, u32[]{:S(2)}, u32[]{:S(2)}) collective-permute-start(bf16[30,256]{1,0:T(8,128)(2,1)S(1)} %slice.248), channel_id=1, source_target_pairs={{0,4},{4,8},{8,12},{12,16},{16,20},{20,24},{24,28},{1,5},{5,9},{9,... | collective-permute-start | bytes 46088 | tf_op jit(solution)/shard_map/ppermute | solution.py:21
  120.4 1.6 copy-start.1
  123.2 4.5 %copy-start.5 = (f32[1024,256]{1,0:T(8,128)S(1)}, f32[1024,256]{1,0:T(8,128)}, u32[]{:S(2)}) copy-start(f32[1024,256]{1,0:T(8,128)} %get-tuple-element.15) | copy-start | bytes 3145732
  123.2 4.5 %copy-start.12 = (bf16[256,2048]{1,0:T(8,128)(2,1)S(1)}, bf16[256,2048]{1,0:T(8,128)(2,1)}, u32[]{:S(2)}) copy-start(bf16[256,2048]{1,0:T(8,128)(2,1)} %param.33) | copy-start | bytes 3145732
  123.2 4.5 %copy-start.15 = (f32[256]{0:T(256)S(1)}, f32[256]{0:T(256)}, u32[]{:S(2)}) copy-start(f32[256]{0:T(256)} %param.31) | copy-start | bytes 3076
  123.2 4.5 %copy-start.16 = (f32[256]{0:T(256)S(1)}, f32[256]{0:T(256)}, u32[]{:S(2)}) copy-start(f32[256]{0:T(256)} %param.30) | copy-start | bytes 3076
Sparse Core Ops, SparseCore 0:
  8.9 37.1 all-gather.3
  71.4 48.9 all-gather.5
  139.4 44.9 reduce-scatter.1

commit v2 on v1

--- a/solution.py
+++ b/solution.py
@@ -8,6 +8,8 @@
 from jax.sharding import PartitionSpec as P
 
 BLOCK = 128
+CHUNKS = 4
+CUTS = 4
 
 
 TINY_NORM = 1e-06
@@ -32,8 +34,8 @@
 
 
 def delta_kernel(
-    heads, width, q_ref, k_ref, v_ref, g_ref, outa_ref, outb_ref, state_ref,
-    lhs_s, corr_s, score_s, wt_s, tail_s,
+    heads, width, q_ref, k_ref, v_ref, g_ref, outa_ref, outb_ref, final_ref,
+    lhs_s, corr_s, score_s, wt_s, tail_s, state_ref,
 ):
     rows = q_ref.shape[0]
     blocks = rows // BLOCK
@@ -121,6 +123,7 @@
         return carry
 
     lax.fori_loop(0, blocks, advance, 0)
+    final_ref[...] = state_ref[...].astype(jnp.bfloat16)
 
 
 def delta_rule(query_raw, key_raw, value_raw, gates, heads, width):
@@ -132,7 +135,7 @@
         out_shape=(
             jax.ShapeDtypeStruct((heads, rows, width), jnp.bfloat16),
             jax.ShapeDtypeStruct((heads, rows, width), jnp.float32),
-            jax.ShapeDtypeStruct((heads, width, 2 * width), jnp.float32),
+            jax.ShapeDtypeStruct((heads, width, 2 * width), jnp.bfloat16),
         ),
         in_specs=[vm] * 4,
         out_specs=(vm, vm, vm),
@@ -142,6 +145,7 @@
             pltpu.VMEM((heads, rows, BLOCK), jnp.bfloat16),
             pltpu.VMEM((heads, blocks, width, BLOCK), jnp.bfloat16),
             pltpu.VMEM((heads, blocks, 8, BLOCK), jnp.float32),
+            pltpu.VMEM((heads, width, 2 * width), jnp.float32),
         ],
         compiler_params=pltpu.CompilerParams(
             vmem_limit_bytes=40 * 1024 * 1024
@@ -161,16 +165,11 @@
 
     def hop(i, carry):
         moved = [
-            jnp.dot(
-                all_ref[i, h, :, :width],
-                carry_s[h],
-                precision=HIGHEST,
-                preferred_element_type=jnp.float32,
-            )
+            mm(all_ref[i, h, :, :width], carry_s[h])
             for h in range(heads)
         ]
         for h in range(heads):
-            carry_s[h] = moved[h] + all_ref[i, h, :, width:]
+            carry_s[h] = moved[h] + all_ref[i, h, :, width:].astype(jnp.float32)
         return carry
 
     lax.fori_loop(0, place_ref[0], hop, 0)
@@ -208,6 +207,270 @@
         ),
         name="delta_finish",
     )(place, states, outa, outb, gate, gain)
+
+
+MESH = pl.DeviceIdType.MESH
+
+
+def sharded_place():
+    tp = lax.axis_size("tp")
+    me = lax.axis_index("tp")
+    core = lax.rem(me, 2)
+    return tp // 2, me, core, me // 2, me + 1 - 2 * core
+
+
+def greet(chips, core, chip, sibling):
+    barrier = pltpu.get_barrier_semaphore()
+    pl.semaphore_signal(barrier, inc=1, device_id={"tp": sibling}, device_id_type=MESH)
+    for o in range(1, chips):
+        there = lax.rem(chip + o, chips) * 2 + core
+        pl.semaphore_signal(barrier, inc=1, device_id={"tp": there}, device_id_type=MESH)
+    pl.semaphore_wait(barrier, chips)
+
+
+def project_kernel(heads, *refs):
+    count = 7
+    tok_ref, w_refs, wg_ref, rate_ref = refs[0], refs[1 : 1 + count], refs[8], refs[9]
+    out_refs, gates_ref = refs[10 : 10 + count], refs[17]
+    full, y_send, y_recv, own_send, own_recv, fwd_send, fwd_recv = refs[18:]
+    rows, part = tok_ref.shape
+    step = rows // CHUNKS
+    chips, me, core, chip, sibling = sharded_place()
+
+    def columns(owner):
+        return pl.ds(pl.multiple_of(owner * part, part), part)
+
+    def at(r):
+        return pl.ds(pl.multiple_of(r * step, step), step)
+
+    def across(o, r):
+        there = lax.rem(chip + o, chips) * 2 + core
+        return pltpu.make_async_remote_copy(
+            src_ref=tok_ref.at[at(r), :],
+            dst_ref=full.at[at(r), columns(me)],
+            send_sem=y_send.at[o - 1, r],
+            recv_sem=y_recv.at[o - 1, r],
+            device_id={"tp": there},
+            device_id_type=MESH,
+        )
+
+    def beside(r):
+        return pltpu.make_async_remote_copy(
+            src_ref=tok_ref.at[at(r), :],
+            dst_ref=full.at[at(r), columns(me)],
+            send_sem=own_send.at[r],
+            recv_sem=own_recv.at[r],
+            device_id={"tp": sibling},
+            device_id_type=MESH,
+        )
+
+    def forward(o, r):
+        owner = lax.rem(chip - o + chips, chips) * 2 + core
+        block = full.at[at(r), columns(owner)]
+        return pltpu.make_async_remote_copy(
+            src_ref=block,
+            dst_ref=block,
+            send_sem=fwd_send.at[o - 1, r],
+            recv_sem=fwd_recv.at[o - 1, r],
+            device_id={"tp": sibling},
+            device_id_type=MESH,
+        )
+
+    greet(chips, core, chip, sibling)
+    for r in range(CHUNKS):
+        for o in range(1, chips):
+            across(o, r).start()
+    for r in range(CHUNKS):
+        beside(r).start()
+    full[:, columns(me)] = tok_ref[...]
+
+    def chunk(r, carry):
+        for o in range(1, chips):
+            across(o, r).wait_recv()
+            forward(o, r).start()
+        beside(r).wait_recv()
+        for o in range(1, chips):
+            forward(o, r).wait_recv()
+        squares = jnp.zeros((step, 1), jnp.float32)
+        for b in range(2 * chips):
+            piece = full[at(r), b * part : (b + 1) * part].astype(jnp.float32)
+            squares = squares + jnp.sum(piece * piece, axis=1, keepdims=True)
+        inv_rms = lax.rsqrt(squares / (part * 2 * chips) + TINY_NORM)
+        for w_ref, out_ref in zip(w_refs, out_refs):
+            summed = jnp.dot(full[at(r), :], w_ref[...], preferred_element_type=jnp.float32)
+            out_ref[at(r), :] = (summed * inv_rms).astype(jnp.bfloat16)
+        raw = jnp.dot(full[at(r), :], wg_ref[...], preferred_element_type=jnp.float32) * inv_rms
+        lane = lax.broadcasted_iota(jnp.int32, raw.shape, 1)
+        softplus = jnp.maximum(raw, 0.0) + jnp.log1p(jnp.exp(-jnp.abs(raw)))
+        gates_ref[at(r), :] = jnp.where(lane < heads, jax.nn.sigmoid(raw), -rate_ref[...] * softplus)
+        return carry
+
+    lax.fori_loop(0, CHUNKS, chunk, 0)
+    for r in range(CHUNKS):
+        for o in range(1, chips):
+            across(o, r).wait_send()
+            forward(o, r).wait_send()
+        beside(r).wait_send()
+
+
+def project(tokens, weights, w_gates, rates, heads):
+    rows, part = tokens.shape
+    tp = lax.axis_size("tp")
+    others = max(tp // 2 - 1, 1)
+    vm = pl.BlockSpec(memory_space=pltpu.VMEM)
+    dma = pltpu.SemaphoreType.DMA
+    return pl.pallas_call(
+        functools.partial(project_kernel, heads),
+        out_shape=tuple(
+            jax.ShapeDtypeStruct((rows, w.shape[1]), jnp.bfloat16) for w in weights
+        )
+        + (jax.ShapeDtypeStruct((rows, w_gates.shape[1]), jnp.float32),),
+        in_specs=[vm] * (3 + len(weights)),
+        out_specs=(vm,) * (1 + len(weights)),
+        scratch_shapes=[
+            pltpu.VMEM((rows, part * tp), jnp.bfloat16),
+            dma((others, CHUNKS)),
+            dma((others, CHUNKS)),
+            dma((CHUNKS,)),
+            dma((CHUNKS,)),
+            dma((others, CHUNKS)),
+            dma((others, CHUNKS)),
+        ],
+        compiler_params=pltpu.CompilerParams(
+            collective_id=0, has_side_effects=True, vmem_limit_bytes=48 * 1024 * 1024
+        ),
+        cost_estimate=pl.CostEstimate(
+            flops=10_000_000_000, bytes_accessed=20_000_000, transcendentals=0
+        ),
+        name="gather_project",
+    )(tokens, *weights, w_gates, rates)
+
+
+def output_kernel(
+    dm_ref, cm_ref, wd_ref, wc_ref, out_ref,
+    beside_out, beside_in, across_out, across_in, b_send, b_recv, y_send, y_recv,
+):
+    chips, me, core, chip, sibling = sharded_place()
+    rows = out_ref.shape[0]
+    width = out_ref.shape[1] // CUTS
+
+    def cols(n):
+        return pl.ds(pl.multiple_of(n * width, width), width)
+
+    def partial(target, n):
+        at = pl.ds(pl.multiple_of(target * rows, rows), rows)
+        summed = jnp.dot(dm_ref[at, :], wd_ref[:, cols(n)], preferred_element_type=jnp.float32)
+        return summed + jnp.dot(
+            cm_ref[at, :], wc_ref[:, cols(n)], preferred_element_type=jnp.float32
+        )
+
+    def beside(o, n):
+        return pltpu.make_async_remote_copy(
+            src_ref=beside_out.at[o, n],
+            dst_ref=beside_in.at[o, n],
+            send_sem=b_send.at[o, n],
+            recv_sem=b_recv.at[o, n],
+            device_id={"tp": sibling},
+            device_id_type=MESH,
+        )
+
+    def across(o, n):
+        there = lax.rem(chip + o, chips) * 2 + core
+        return pltpu.make_async_remote_copy(
+            src_ref=across_out.at[o - 1, n],
+            dst_ref=across_in.at[o - 1, n],
+            send_sem=y_send.at[o - 1, n],
+            recv_sem=y_recv.at[o - 1, n],
+            device_id={"tp": there},
+            device_id_type=MESH,
+        )
+
+    greet(chips, core, chip, sibling)
+    order = list(range(1, chips)) + [0]
+    for o in order:
+        their_chip = lax.rem(chip + o, chips) * 2
+
+        def give(n, carry, o=o, their_chip=their_chip):
+            beside_out[o, n] = partial(their_chip + 1 - core, n).astype(jnp.bfloat16)
+            beside(o, n).start()
+            return carry
+
+        def keep(n, carry, o=o, their_chip=their_chip):
+            mine = partial(their_chip + core, n)
+            beside(o, n).wait_recv()
+            mine = mine + beside_in[o, n].astype(jnp.float32)
+            across_out[o - 1, n] = mine.astype(jnp.bfloat16)
+            across(o, n).start()
+            return carry
+
+        if o != 0:
+
+            def both(n, carry, give=give, keep=keep):
+                @pl.when(n + 1 < CUTS)
+                def _():
+                    give(n + 1, 0)
+
+                return keep(n, carry)
+
+            give(0, 0)
+            lax.fori_loop(0, CUTS, both, 0)
+        else:
+            lax.fori_loop(0, CUTS, give, 0)
+
+    def close(n, carry):
+        mine = partial(me, n)
+        beside(0, n).wait_recv()
+        mine = mine + beside_in[0, n].astype(jnp.float32)
+        for o in range(1, chips):
+            across(o, n).wait_recv()
+            mine = mine + across_in[o - 1, n].astype(jnp.float32)
+        out_ref[:, cols(n)] = mine.astype(jnp.bfloat16)
+        return carry
+
+    lax.fori_loop(0, CUTS, close, 0)
+
+    def drain(n, carry):
+        for o in range(chips):
+            beside(o, n).wait_send()
+        for o in range(1, chips):
+            across(o, n).wait_send()
+        return carry
+
+    lax.fori_loop(0, CUTS, drain, 0)
+
+
+def output_projection(delta_mixed, conv_mixed, out_delta, out_conv):
+    tp = lax.axis_size("tp")
+    chips = tp // 2
+    others = max(chips - 1, 1)
+    rows = delta_mixed.shape[0] // tp
+    width = out_delta.shape[1]
+    cut = width // CUTS
+    vm = pl.BlockSpec(memory_space=pltpu.VMEM)
+    dma = pltpu.SemaphoreType.DMA
+    return pl.pallas_call(
+        output_kernel,
+        out_shape=jax.ShapeDtypeStruct((rows, width), jnp.bfloat16),
+        in_specs=[vm] * 4,
+        out_specs=vm,
+        scratch_shapes=[
+            pltpu.VMEM((chips, CUTS, rows, cut), jnp.bfloat16),
+            pltpu.VMEM((chips, CUTS, rows, cut), jnp.bfloat16),
+            pltpu.VMEM((others, CUTS, rows, cut), jnp.bfloat16),
+            pltpu.VMEM((others, CUTS, rows, cut), jnp.bfloat16),
+            dma((chips, CUTS)),
+            dma((chips, CUTS)),
+            dma((others, CUTS)),
+            dma((others, CUTS)),
+        ],
+        compiler_params=pltpu.CompilerParams(
+            collective_id=1, has_side_effects=True, vmem_limit_bytes=48 * 1024 * 1024
+        ),
+        cost_estimate=pl.CostEstimate(
+            flops=10_000_000_000, bytes_accessed=20_000_000, transcendentals=0
+        ),
+        name="output_scatter",
+    )(delta_mixed, conv_mixed, out_delta, out_conv)
 
 
 def local(
@@ -231,45 +494,33 @@
 ):
     rows_here = tokens.shape[0]
     tp_size = lax.axis_size("tp")
-    width_all = tokens.shape[1] * tp_size
-    weights = (
-        w_query,
-        w_key,
-        w_value,
-        w_delta_gate,
-        w_glu_value,
-        w_glu_gate,
-        w_conv_gate,
-        w_beta,
-        w_decay,
-    )
-    piece = lax.all_gather(tokens, "tp", axis=1, tiled=True)
-    totals = tuple(
-        (jnp.dot(piece, weight, preferred_element_type=jnp.float32) for weight in weights)
-    )
-    squares = jnp.sum(jnp.square(piece.astype(jnp.float32)), axis=1)
-    sums, squares = (totals, squares)
-    inv_rms = lax.rsqrt(squares / width_all + TINY_NORM)[:, None]
-    scaled = [summed * inv_rms for summed in sums]
-    query_raw, key_raw, value_raw, delta_gate_raw, glu_value_raw, glu_gate_raw, conv_gate_raw = [
-        item.astype(jnp.bfloat16) for item in scaled[:7]
-    ]
     head_size = head_gain.shape[0]
     heads_here = w_query.shape[1] // head_size
     first_head = lax.axis_index("tp") * heads_here
-    strength = jax.nn.sigmoid(lax.dynamic_slice_in_dim(scaled[7], first_head, heads_here, 1))
     rates = jnp.exp(lax.dynamic_slice_in_dim(decay_log, first_head, heads_here, 0))
-    log_decay = -rates[None, :] * jax.nn.softplus(
-        lax.dynamic_slice_in_dim(scaled[8], first_head, heads_here, 1)
-    )
-    gates = jnp.concatenate(
+    fill = head_size - 2 * heads_here
+    rates = jnp.concatenate(
+        [jnp.zeros((heads_here,), jnp.float32), rates, jnp.zeros((fill,), jnp.float32)]
+    )[None, :]
+    w_gates = jnp.concatenate(
         [
-            strength,
-            log_decay,
-            jnp.zeros((rows_here, head_size - 2 * heads_here), jnp.float32),
+            lax.dynamic_slice_in_dim(w_beta, first_head, heads_here, 1),
+            lax.dynamic_slice_in_dim(w_decay, first_head, heads_here, 1),
+            jnp.zeros((w_beta.shape[0], fill), jnp.bfloat16),
         ],
         axis=1,
     )
+    weights = (w_query, w_key, w_value, w_delta_gate, w_glu_value, w_glu_gate, w_conv_gate)
+    (
+        query_raw,
+        key_raw,
+        value_raw,
+        delta_gate_raw,
+        glu_value_raw,
+        glu_gate_raw,
+        conv_gate_raw,
+        gates,
+    ) = project(tokens, weights, w_gates, rates, heads_here)
     outa, outb, final = delta_rule(
         query_raw, key_raw, value_raw, gates, heads_here, head_size
     )
@@ -302,15 +553,7 @@
     conv_mixed = (jax.nn.silu(normed) * jax.nn.silu(conv_gate_raw.astype(jnp.float32))).astype(
         jnp.bfloat16
     )
-    summed = jnp.dot(delta_mixed, out_delta, preferred_element_type=jnp.float32)
-    return lax.psum_scatter(
-        (summed + jnp.dot(conv_mixed, out_conv, preferred_element_type=jnp.float32)).astype(
-            jnp.bfloat16
-        ),
-        "tp",
-        scatter_dimension=0,
-        tiled=True,
-    )
+    return output_projection(delta_mixed, conv_mixed, out_delta, out_conv)
 
 
 def solution(mesh):

time: 191 us -> 140 us (0.73)
  waiting for transfers between devices: 111 us -> 23.8 us
  Pallas kernels: 15.9 us -> 76.9 us
  matrix products: 28.7 us -> 0 us
  local copies, waits for them, and re-layouts: 2.05 us -> 6.42 us
  other arithmetic: 10.6 us -> 8.55 us
    pallas_call x0 -> x2, Pallas kernels: none -> 61 us  [the longest x1 33.5 us: project(): pl.pallas_call(functools.partial(project_kernel, heads), out_shape=tuple(...]
    reduce_scatter x1 -> x0, waiting for transfers between devices: 45.1 us -> none  [local(): lax.psum_scatter((summed + jnp.dot(conv_mixed, out_conv, preferred_elemen...]
    all_gather x1 -> x0, waiting for transfers between devices: 38 us -> none  [local(): piece = lax.all_gather(tokens, 'tp', axis=1, tiled=True)]
    dot_general x10 -> x0, matrix products: 28.7 us -> none  [the longest x8 12.6 us: local(): jnp.dot(piece, weight, preferred_element_type=jnp.float32)]
    unnamed x34 -> x21, local copies, waits for them, and re-layouts: 1.96 us -> 5.46 us
    reduce_sum x1 -> x0, other arithmetic: 3.22 us -> none  [local(): squares = jnp.sum(jnp.square(piece.astype(jnp.float32)), axis=1)]
    all_gather x1, waiting for transfers between devices: 26.6 us -> 23.8 us  [local(): states = lax.all_gather(final, 'sp')]
    convert_element_type x0 -> x2, other arithmetic: none -> 2.15 us  [the longest x1 1.86 us: local(): (jax.nn.silu(normed) * jax.nn.silu(conv_gate_raw.astype(jnp.float32))).as...]
  transfers between devices with their start and end apart: 4 -> 2, of which waited for: 4 -> 1; matrix products, arithmetic and copies ran while one was open for 7% -> 6% of each run, Pallas kernels for 0% -> 10%
where the time goes in v2:
time: 140 us
  Pallas kernels  76.9 us (55%)
  waiting for transfers between devices  23.8 us (17%)
  between operations  13.6 us (10%)
  other arithmetic  8.55 us (6%)
  blocking collectives  7.62 us (5%)
  local copies, waits for them, and re-layouts  6.42 us (5%)
  starting transfers between devices  2.89 us (2%)
    pallas_call x1, Pallas kernels, project(): pl.pallas_call(functools.partial(project_kernel, heads), out_shape=tuple(...  33.5 us
    pallas_call x1, Pallas kernels, output_projection(): pl.pallas_call(output_kernel, out_shape=jax.ShapeDtypeStruct((rows, width...  27.5 us
    all_gather x1, waiting for transfers between devices, local(): states = lax.all_gather(final, 'sp')  23.8 us
    pallas_call x1, Pallas kernels, delta_rule(): pl.pallas_call(functools.partial(delta_kernel, heads, width), out_shape=(...  14.6 us
    psum x1, blocking collectives, local(): first_sum, second_sum = lax.psum((first_sum, second_sum), 'tp')  7.62 us
    reduce_sum x1, other arithmetic, local(): first_sum = jnp.sum(filtered, axis=1)  5.96 us
    unnamed x21, local copies, waits for them, and re-layouts  5.46 us
    ppermute x1, starting transfers between devices, shifted(): return lax.ppermute(block, axis, route)  2.89 us
  transfers between devices with their start and end apart: 2, of which 1 were waited for; matrix products, arithmetic and copies ran while one was open for 6% of the time, Pallas kernels for 10%

profile of v2, /device:TPU:0, one launch (start us, length us, event | category | flops | bytes accessed | tf_op | source)
XLA Modules:
  0.0 139.7 jit_solution(10389152233770678112)
XLA Ops:
  6.5 0.0 all-gather.3.cloned.1.call-start
  6.5 0.8 constant_dynamic-slice_fusion
  7.3 0.0 copy-start.8
  7.3 0.3 copy.22
  7.7 0.0 copy-start
  7.7 0.3 copy.23
  8.0 0.0 copy-done.8
  8.0 0.1 dynamic-slice_exponential_fusion
  8.1 0.1 pad.7.clone
  8.2 0.3 maximum_maximum_fusion.refs_8_
  8.5 0.1 maximum_bitcast_fusion.refs_9_
  8.6 0.3 copy-done
  8.9 33.5 %gather_project.1 = (bf16[1024,256]{1,0:T(8,128)(2,1)S(1)}, bf16[1024,256]{1,0:T(8,128)(2,1)S(1)}, bf16[1024,256]{1,0:T(8,128)(2,1)S(1)}, bf16[1024,256]{1,0:T(8...) custom-call(bf16[1024,512]{1,0:T(8,128)(2,1)S(1)} %copy-done, ...), custom_call_target="tpu_custom_call" | custom-call | flops 10000000000 | bytes 20000000 | tf_op jit(solution)/shard_map/gather_project/pallas_call | solution.py:322
  42.4 0.3 multiply_convert_fusion
  42.7 2.9 %collective-permute-start = (bf16[30,256]{1,0:T(8,128)(2,1)S(1)}, bf16[30,256]{1,0:T(8,128)(2,1)S(1)}, u32[]{:S(2)}, u32[]{:S(2)}) collective-permute-start(bf16[30,256]{1,0:T(8,128)(2,1)S(1)} %slice.248), channel_id=1, source_target_pairs={{0,4},{4,8},{8,12},{12,16},{16,20},{20,24},{24,28},{1,5},{5,9},{9,... | collective-permute-start | bytes 46088 | tf_op jit(solution)/shard_map/ppermute | solution.py:23
  45.6 14.6 %delta_rule.1 = (bf16[2,1024,128]{2,1,0:T(8,128)(2,1)S(1)}, f32[2,1024,128]{2,1,0:T(8,128)S(1)}, bf16[2,128,256]{2,1,0:T(8,128)(2,1)}) custom-call(bf16[1024,256]{1,0:T(8,128)(2,1)S(1)} %get-tuple-element.16.q_ref, bf16[1024,256]{1,0:T(8,128)(2,1)S(1)} %get-tuple-element.17.k_ref, bf16[1024,256]{1,0:T(8,128)(2,1)S(1)} %get-tuple-element.18.v_ref, ...), custom_call_target="tpu_custom_call" | custom-call | flops 10000000000 | bytes 4000000 | tf_op jit(solution)/shard_map/delta_rule/pallas_call | solution.py:133
  60.2 0.0 copy-start.5
  60.2 0.0 all-gather.3.cloned.1.call-update
  60.3 0.7 copy-done.5
  61.0 0.0 collective-permute-done
  61.0 0.0 copy-start.7
  61.0 6.0 %fusion.34 = (f32[1024]{0:T(1024)S(1)}, f32[1024]{0:T(1024)S(1)}, f32[1024,256]{1,0:T(8,128)}) fusion(f32[256]{0:T(256)S(1)} %bitcast.67, bf16[1024,256]{1,0:T(8,128)(2,1)S(1)} %multiply_convert_fusion, f32[256]{0:T(256)S(1)} %bitcast.68, bf16[30,256]{1,0:T(8,128)(2,1)S(1)} %collective-permute-done, f32[256]{0:T(256)S(1)} %bitcast.39, f32[256]{0:T(256)S(1)} %bitcast.40, ...), kind=kLoop, calls=%fused_computation.111 | loop fusion | flops 48494592 | bytes 1628160 | tf_op jit(solution)/shard_map/reduce_sum | solution.py:544
  67.0 7.6 %all-reduce = (f32[1024]{0:T(1024)S(1)}, f32[1024]{0:T(1024)S(1)}) all-reduce(f32[1024]{0:T(1024)S(1)} %get-tuple-element.28, f32[1024]{0:T(1024)S(1)} %get-tuple-element.27), channel_id=1, replica_groups=mesh['sp'=8,'tp'=4] {'tp'}, use_global_device_ids=true, to_apply=%region_3.0 | all-reduce | flops 2048 | bytes 16384 | tf_op jit(solution)/shard_map/psum | solution.py:546
  74.6 0.0 copy-start.6
  74.6 0.0 copy-done.7
  74.6 0.7 copy-done.6
  75.3 1.9 %fusion.4.cm_ref = bf16[1024,256]{1,0:T(8,128)(2,1)S(1)} fusion(bf16[1024,256]{1,0:T(8,128)(2,1)S(1)} %get-tuple-element.26, f32[1024,256]{1,0:T(8,128)} %get-tuple-element.31, f32[256]{0:T(256)S(1)} %copy-done.6, f32[256]{0:T(256)S(1)} %copy-done.7, f32[1024]{0:T(1024)S(1)} %get-tuple-element.64, f32[1024]{0:T(1024)S(1)} %get-tuple-element.63), kind=kLoop, calls=%fused_computation.38 | loop fusion | flops 3932160 | bytes 2107392 | tf_op jit(solution)/shard_map/convert_element_type | solution.py:553
  77.2 23.8 %all-gather.3.cloned.1.call-done = bf16[16,128,256]{2,1,0:T(8,128)(2,1)} async-done(((bf16[2,128,256]{2,1,0:T(8,128)(2,1)}), bf16[16,128,256]{2,1,0:T(8,128)(2,1)}) %all-gather.3.cloned.1.call-update) | async-done | bytes 1048592 | tf_op jit(solution)/shard_map/all_gather | solution.py:527
  101.0 0.0 copy-start.4
  101.0 0.7 copy-done.4
  101.6 0.0 copy-start.3
  101.6 1.2 copy-done.3
  102.9 0.0 copy-start.1
  102.9 0.0 copy-start.2
  102.9 1.2 delta_finish.1.dm_ref
  104.1 0.0 copy-done.1
  104.1 0.3 copy-done.2
  104.4 27.5 %output_scatter.1 = bf16[256,2048]{1,0:T(8,128)(2,1)S(1)} custom-call(bf16[1024,256]{1,0:T(8,128)(2,1)S(1)} %delta_finish.1.dm_ref, bf16[1024,256]{1,0:T(8,128)(2,1)S(1)} %fusion.4.cm_ref, bf16[256,2048]{1,0:T(8,128)(2,1)S(1)} %copy-done.1, bf16[256,2048]{1,0:T(8,128)(2,1)S(1)} %copy-done.2), custom_call_target="tpu_custom_call" | custom-call | flops 10000000000 | bytes 20000000 | tf_op jit(solution)/shard_map/output_scatter/pallas_call | solution.py:451
  131.9 1.0 copy.25
  (7 shorter events, 0.1 us)
Async XLA Ops:
  6.5 94.4 %all-gather.3.cloned.1.call-start = ((), (), s32[]{:S(2)}) async-start(), calls=%async_computation | async-start | bytes 1179648 | tf_op jit(solution)/shard_map/all_gather | solution.py:527
  7.3 0.7 copy-start.8
  7.7 1.2 copy-start
  42.7 18.3 %collective-permute-start = (bf16[30,256]{1,0:T(8,128)(2,1)S(1)}, bf16[30,256]{1,0:T(8,128)(2,1)S(1)}, u32[]{:S(2)}, u32[]{:S(2)}) collective-permute-start(bf16[30,256]{1,0:T(8,128)(2,1)S(1)} %slice.248), channel_id=1, source_target_pairs={{0,4},{4,8},{8,12},{12,16},{16,20},{20,24},{24,28},{1,5},{5,9},{9,... | collective-permute-start | bytes 46088 | tf_op jit(solution)/shard_map/ppermute | solution.py:23
  60.2 0.7 copy-start.5
  61.0 13.6 %copy-start.7 = (f32[256]{0:T(256)S(1)}, f32[256]{0:T(256)}, u32[]{:S(2)}) copy-start(f32[256]{0:T(256)} %param.30) | copy-start | bytes 3076
  74.6 0.7 copy-start.6
  101.0 0.7 copy-start.4
  101.6 1.2 copy-start.3
  102.9 1.2 copy-start.1
  102.9 1.5 %copy-start.2 = (bf16[256,2048]{1,0:T(8,128)(2,1)S(1)}, bf16[256,2048]{1,0:T(8,128)(2,1)}, u32[]{:S(2)}) copy-start(bf16[256,2048]{1,0:T(8,128)(2,1)} %wc_ref.1) | copy-start | bytes 3145732
Sparse Core Ops, SparseCore 0:
  60.4 40.5 all-gather.2

commit v3 on v2

--- a/solution.py
+++ b/solution.py
@@ -21,6 +21,29 @@
     devices = range(lax.axis_size(axis))
     route = [(i - distance, i) for i in devices if i - distance in devices]
     return lax.ppermute(block, axis, route)
+
+
+def compose(later, earlier, width):
+    moved = jnp.einsum(
+        "hij,hjk->hik",
+        later[..., :width].astype(jnp.bfloat16),
+        earlier,
+        preferred_element_type=jnp.float32,
+    )
+    return moved + jnp.concatenate(
+        [jnp.zeros_like(later[..., :width]), later[..., width:]], axis=-1
+    ).astype(jnp.float32)
+
+
+def entering(final, axis, width):
+    devices = lax.axis_size(axis)
+    window = compose(shifted(final, axis, 1), shifted(final, axis, 2), width)
+    reach = 2
+    while 2 * reach < devices:
+        earlier = shifted(window.astype(jnp.bfloat16), axis, reach)
+        window = compose(window, earlier, width)
+        reach *= 2
+    return window, shifted(window[..., width:].astype(jnp.bfloat16), axis, reach)
 
 
 def nt(a, b):
@@ -158,28 +181,21 @@
 
 
 def finish_kernel(
-    heads, width, place_ref, all_ref, outa_ref, outb_ref, gate_ref, gain_ref, mixed_ref, carry_s
+    heads, width, window_ref, earlier_ref, outa_ref, outb_ref, gate_ref, gain_ref, mixed_ref
 ):
     rows = outb_ref.shape[1]
-    carry_s[...] = jnp.zeros_like(carry_s)
-
-    def hop(i, carry):
-        moved = [
-            mm(all_ref[i, h, :, :width], carry_s[h])
-            for h in range(heads)
-        ]
-        for h in range(heads):
-            carry_s[h] = moved[h] + all_ref[i, h, :, width:].astype(jnp.float32)
-        return carry
-
-    lax.fori_loop(0, place_ref[0], hop, 0)
+    carried = [
+        mm(window_ref[h, :, :width], earlier_ref[h]) + window_ref[h, :, width:]
+        for h in range(heads)
+    ]
+    carried = [item.astype(jnp.bfloat16) for item in carried]
     tile = 256
 
     def one(c, carry):
         at = pl.ds(pl.multiple_of(c * tile, tile), tile)
         for h in range(heads):
             lanes = slice(h * width, (h + 1) * width)
-            result = outb_ref[h, at, :] + mm(outa_ref[h, at, :], carry_s[h])
+            result = outb_ref[h, at, :] + mm(outa_ref[h, at, :], carried[h])
             result = result * lax.rsqrt(
                 jnp.mean(result * result, axis=-1, keepdims=True) + TINY_NORM
             )
@@ -192,21 +208,20 @@
     lax.fori_loop(0, rows // tile, one, 0)
 
 
-def finish(place, states, outa, outb, gate, gain, heads, width):
+def finish(window, earlier, outa, outb, gate, gain, heads, width):
     rows = outb.shape[1]
     vm = pl.BlockSpec(memory_space=pltpu.VMEM)
     return pl.pallas_call(
         functools.partial(finish_kernel, heads, width),
         out_shape=jax.ShapeDtypeStruct((rows, heads * width), jnp.bfloat16),
-        in_specs=[pl.BlockSpec(memory_space=pltpu.SMEM)] + [vm] * 5,
+        in_specs=[vm] * 6,
         out_specs=vm,
-        scratch_shapes=[pltpu.VMEM((heads, width, width), jnp.float32)],
         compiler_params=pltpu.CompilerParams(vmem_limit_bytes=40 * 1024 * 1024),
         cost_estimate=pl.CostEstimate(
             flops=2_000_000_000, bytes_accessed=6_000_000, transcendentals=0
         ),
         name="delta_finish",
-    )(place, states, outa, outb, gate, gain)
+    )(window, earlier, outa, outb, gate, gain)
 
 
 MESH = pl.DeviceIdType.MESH
@@ -524,10 +539,9 @@
     outa, outb, final = delta_rule(
         query_raw, key_raw, value_raw, gates, heads_here, head_size
     )
-    states = lax.all_gather(final, "sp")
-    place = lax.axis_index("sp").astype(jnp.int32).reshape(1)
+    window, earlier = entering(final, "sp", head_size)
     delta_mixed = finish(
-        place, states, outa, outb, delta_gate_raw, head_gain[None, :], heads_here, head_size
+        window, earlier, outa, outb, delta_gate_raw, head_gain[None, :], heads_here, head_size
     )
     kernel = conv_taps.shape[0]
     channels = conv_taps.shape[1]

time: 140 us -> 119 us (0.85)
  waiting for transfers between devices: 23.8 us -> 4.56 us
  starting transfers between devices: 2.89 us -> 20.2 us
  between operations: 13.6 us -> 0.3 us
  local copies, waits for them, and re-layouts: 6.42 us -> 4.39 us
  blocking collectives: 7.62 us -> 6.09 us
    all_gather x1 -> x0, waiting for transfers between devices: 23.8 us -> none  [local(): states = lax.all_gather(final, 'sp')]
    ppermute x1 -> x5, starting transfers between devices: 2.89 us -> 20.2 us  [shifted(): return lax.ppermute(block, axis, route)]
    ppermute x1 -> x5, waiting for transfers between devices: 0.01 us -> 4.56 us  [shifted(): return lax.ppermute(block, axis, route)]
    unnamed x21, local copies, waits for them, and re-layouts: 5.46 us -> 3.4 us
    psum x1, blocking collectives: 7.62 us -> 6.09 us  [local(): first_sum, second_sum = lax.psum((first_sum, second_sum), 'tp')]
  transfers between devices with their start and end apart: 2 -> 5, of which waited for: 1 -> 3; matrix products, arithmetic and copies ran while one was open for 6% -> 6% of each run, Pallas kernels for 10% -> 0%
where the time goes in v3:
time: 119 us
  Pallas kernels  75.9 us (64%)
  starting transfers between devices  20.2 us (17%)
  other arithmetic  7.26 us (6%)
  blocking collectives  6.09 us (5%)
  waiting for transfers between devices  4.56 us (4%)
  local copies, waits for them, and re-layouts  4.39 us (4%)
    pallas_call x1, Pallas kernels, project(): pl.pallas_call(functools.partial(project_kernel, heads), out_shape=tuple(...  33.5 us
    pallas_call x1, Pallas kernels, output_projection(): pl.pallas_call(output_kernel, out_shape=jax.ShapeDtypeStruct((rows, width...  27 us
    ppermute x5, starting transfers between devices, shifted(): return lax.ppermute(block, axis, route)  20.2 us
    pallas_call x1, Pallas kernels, delta_rule(): pl.pallas_call(functools.partial(delta_kernel, heads, width), out_shape=(...  14 us
    psum x1, blocking collectives, local(): first_sum, second_sum = lax.psum((first_sum, second_sum), 'tp')  6.09 us
    reduce_sum x1, other arithmetic, local(): first_sum = jnp.sum(filtered, axis=1)  5.88 us
    ppermute x5, waiting for transfers between devices, shifted(): return lax.ppermute(block, axis, route)  4.56 us
    unnamed x21, local copies, waits for them, and re-layouts  3.4 us
  transfers between devices with their start and end apart: 5, of which 3 were waited for; matrix products, arithmetic and copies ran while one was open for 6% of the time, Pallas kernels for 0%

profile of v3, /device:TPU:0, one launch (start us, length us, event | category | flops | bytes accessed | tf_op | source)
XLA Modules:
  0.0 119.0 jit_solution(17982962506949868731)
XLA Ops:
  0.0 0.8 constant_dynamic-slice_fusion
  0.8 0.0 copy-start.8
  0.8 0.3 copy.20
  1.1 0.0 copy-start
  1.1 0.3 copy.21
  1.5 0.0 copy-done.8
  1.5 0.1 dynamic-slice_exponential_fusion
  1.5 0.1 pad.9.clone
  1.6 0.3 maximum_maximum_fusion.refs_8_
  2.0 0.1 maximum_bitcast_fusion.refs_9_
  2.1 0.3 copy-done
  2.4 33.5 %gather_project.1 = (bf16[1024,256]{1,0:T(8,128)(2,1)S(1)}, bf16[1024,256]{1,0:T(8,128)(2,1)S(1)}, bf16[1024,256]{1,0:T(8,128)(2,1)S(1)}, bf16[1024,256]{1,0:T(8...) custom-call(bf16[1024,512]{1,0:T(8,128)(2,1)S(1)} %copy-done, ...), custom_call_target="tpu_custom_call" | custom-call | flops 10000000000 | bytes 20000000 | tf_op jit(solution)/shard_map/gather_project/pallas_call | solution.py:337
  35.9 14.0 %delta_rule.1 = (bf16[2,1024,128]{2,1,0:T(8,128)(2,1)S(1)}, f32[2,1024,128]{2,1,0:T(8,128)S(1)}, bf16[2,128,256]{2,1,0:T(8,128)(2,1)S(1)}) custom-call(bf16[1024,256]{1,0:T(8,128)(2,1)S(1)} %get-tuple-element.16.q_ref, bf16[1024,256]{1,0:T(8,128)(2,1)S(1)} %get-tuple-element.17.k_ref, bf16[1024,256]{1,0:T(8,128)(2,1)S(1)} %get-tuple-element.18.v_ref, ...), custom_call_target="tpu_custom_call" | custom-call | flops 10000000000 | bytes 4000000 | tf_op jit(solution)/shard_map/delta_rule/pallas_call | solution.py:156
  49.8 2.9 %collective-permute-start = (bf16[2,128,256]{2,1,0:T(8,128)(2,1)S(1)}, bf16[2,128,256]{2,1,0:T(8,128)(2,1)S(1)}, u32[]{:S(2)}, u32[]{:S(2)}) collective-permute-start(bf16[2,128,256]{2,1,0:T(8,128)(2,1)S(1)} %get-tuple-element.20), channel_id=1, source_target_pairs={{0,4},{4,8},{8,12},{12,16},{16,20},{20,24},{24,28},{1,5},{5,9},{9,... | collective-permute-start | bytes 393224 | tf_op jit(solution)/shard_map/ppermute | solution.py:23
  52.8 3.5 %collective-permute-start.1 = (bf16[2,128,256]{2,1,0:T(8,128)(2,1)S(1)}, bf16[2,128,256]{2,1,0:T(8,128)(2,1)S(1)}, u32[]{:S(2)}, u32[]{:S(2)}) collective-permute-start(bf16[2,128,256]{2,1,0:T(8,128)(2,1)S(1)} %get-tuple-element.20), channel_id=1, source_target_pairs={{0,8},{4,12},{8,16},{12,20},{16,24},{20,28},{1,9},{5,13},{9,17},{1... | collective-permute-start | bytes 393224 | tf_op jit(solution)/shard_map/ppermute | solution.py:23
  56.2 0.3 multiply_convert_fusion
  56.5 0.0 copy-start.5
  56.6 3.4 %collective-permute-start.4 = (bf16[30,256]{1,0:T(8,128)(2,1)S(1)}, bf16[30,256]{1,0:T(8,128)(2,1)S(1)}, u32[]{:S(2)}, u32[]{:S(2)}) collective-permute-start(bf16[30,256]{1,0:T(8,128)(2,1)S(1)} %slice.275), channel_id=1, source_target_pairs={{0,4},{4,8},{8,12},{12,16},{16,20},{20,24},{24,28},{1,5},{5,9},{9,... | collective-permute-start | bytes 46088 | tf_op jit(solution)/shard_map/ppermute | solution.py:23
  60.0 0.0 copy-done.5
  60.1 1.4 %collective-permute-done.4 = bf16[30,256]{1,0:T(8,128)(2,1)S(1)} collective-permute-done((bf16[30,256]{1,0:T(8,128)(2,1)S(1)}, bf16[30,256]{1,0:T(8,128)(2,1)S(1)}, u32[]{:S(2)}, u32[]{:S(2)}) %collective-permute-start.4) | collective-permute-done | bytes 15392 | tf_op jit(solution)/shard_map/ppermute | solution.py:23
  61.5 5.9 %fusion.36 = (f32[1024]{0:T(1024)S(1)}, f32[1024]{0:T(1024)S(1)}, f32[1024,256]{1,0:T(8,128)}) fusion(f32[256]{0:T(256)S(1)} %bitcast.66, bf16[1024,256]{1,0:T(8,128)(2,1)S(1)} %multiply_convert_fusion, f32[256]{0:T(256)S(1)} %bitcast.67, bf16[30,256]{1,0:T(8,128)(2,1)S(1)} %collective-permute-done.4, f32[256]{0:T(256)S(1)} %bitcast.38, ...), kind=kLoop, calls=%fused_computation.116 | loop fusion | flops 48494592 | bytes 1628160 | tf_op jit(solution)/shard_map/reduce_sum | solution.py:558
  67.3 6.1 %all-reduce.2 = (f32[1024]{0:T(1024)S(1)}, f32[1024]{0:T(1024)S(1)}) all-reduce(f32[1024]{0:T(1024)S(1)} %get-tuple-element.28, f32[1024]{0:T(1024)S(1)} %get-tuple-element.27), channel_id=1, replica_groups=mesh['sp'=8,'tp'=4] {'tp'}, use_global_device_ids=true, to_apply=%region_3.0 | all-reduce | flops 2048 | bytes 16384 | tf_op jit(solution)/shard_map/psum | solution.py:560
  73.4 0.0 copy-start.4
  73.4 0.0 collective-permute-done
  73.5 0.0 collective-permute-done.1
  73.5 0.2 fusion.37
  73.7 5.0 %collective-permute-start.2 = (bf16[2,128,256]{2,1,0:T(8,128)(2,1)S(1)}, bf16[2,128,256]{2,1,0:T(8,128)(2,1)S(1)}, u32[]{:S(2)}, u32[]{:S(2)}) collective-permute-start(bf16[2,128,256]{2,1,0:T(8,128)(2,1)S(1)} %get-tuple-element.65), channel_id=1, source_target_pairs={{0,8},{4,12},{8,16},{12,20},{16,24},{20,28},{1,9},{5,13},{9,17},{1... | collective-permute-start | bytes 393224 | tf_op jit(solution)/shard_map/ppermute | solution.py:23
  78.7 0.0 copy-start.7
  78.7 2.6 %collective-permute-done.2 = bf16[2,128,256]{2,1,0:T(8,128)(2,1)S(1)} collective-permute-done((bf16[2,128,256]{2,1,0:T(8,128)(2,1)S(1)}, bf16[2,128,256]{2,1,0:T(8,128)(2,1)S(1)}, u32[]{:S(2)}, u32[]{:S(2)}) %collective-permute-start.2) | collective-permute-done | bytes 131104 | tf_op jit(solution)/shard_map/ppermute | solution.py:23
  81.3 0.2 convolution_add_fusion.window_ref
  81.5 5.4 %collective-permute-start.3 = (bf16[2,128,128]{2,1,0:T(8,128)(2,1)S(1)}, bf16[2,128,128]{2,1,0:T(8,128)(2,1)S(1)}, u32[]{:S(2)}, u32[]{:S(2)}) collective-permute-start(bf16[2,128,128]{2,1,0:T(8,128)(2,1)S(1)} %slice.552), channel_id=1, source_target_pairs={{0,16},{4,20},{8,24},{12,28},{1,17},{5,21},{9,25},{13,29},{2,18},{... | collective-permute-start | bytes 196616 | tf_op jit(solution)/shard_map/ppermute | solution.py:23
  86.9 0.0 copy-start.6
  86.9 0.0 copy-done.4
  86.9 0.0 copy-done.7
  86.9 0.7 copy-done.6
  87.6 0.6 fusion.4.cm_ref
  88.2 0.6 collective-permute-done.3.earlier_ref
  88.8 0.0 copy-start.3
  88.8 0.7 copy-done.3
  89.5 0.0 copy-start.1
  89.5 0.0 copy-start.2
  89.5 1.4 %delta_finish.1.dm_ref = bf16[1024,256]{1,0:T(8,128)(2,1)S(1)} custom-call(f32[2,128,256]{2,1,0:T(8,128)S(1)} %convolution_add_fusion.window_ref, bf16[2,128,128]{2,1,0:T(8,128)(2,1)S(1)} %collective-permute-done.3.earlier_ref, bf16[2,1024,128]{2,1,0:T(8,128)(2,1)S(1)} %get-tuple-element.21.outa_ref, f32[2,1024,128]{2,1,0:T(8,128)S(1)} %get-tuple-element.22.outb_ref, ...), custom_call_target="tpu_custom_call" | custom-call | flops 2000000000 | bytes 6000000 | tf_op jit(solution)/shard_map/delta_finish/pallas_call | solution.py:214
  90.8 0.0 copy-done.1
  90.8 0.2 copy-done.2
  91.0 27.0 %output_scatter.1 = bf16[256,2048]{1,0:T(8,128)(2,1)S(1)} custom-call(bf16[1024,256]{1,0:T(8,128)(2,1)S(1)} %delta_finish.1.dm_ref, bf16[1024,256]{1,0:T(8,128)(2,1)S(1)} %fusion.4.cm_ref, bf16[256,2048]{1,0:T(8,128)(2,1)S(1)} %copy-done.1, bf16[256,2048]{1,0:T(8,128)(2,1)S(1)} %copy-done.2), custom_call_target="tpu_custom_call" | custom-call | flops 10000000000 | bytes 20000000 | tf_op jit(solution)/shard_map/output_scatter/pallas_call | solution.py:466
  118.0 1.0 copy.23
  (10 shorter events, 0.1 us)
Async XLA Ops:
  0.8 0.7 copy-start.8
  1.1 1.2 %copy-start = (bf16[1024,512]{1,0:T(8,128)(2,1)S(1)}, bf16[1024,512]{1,0:T(8,128)(2,1)}, u32[]{:S(2)}) copy-start(bf16[1024,512]{1,0:T(8,128)(2,1)} %refs_0_.1) | copy-start | bytes 3145732
  49.8 23.6 %collective-permute-start = (bf16[2,128,256]{2,1,0:T(8,128)(2,1)S(1)}, bf16[2,128,256]{2,1,0:T(8,128)(2,1)S(1)}, u32[]{:S(2)}, u32[]{:S(2)}) collective-permute-start(bf16[2,128,256]{2,1,0:T(8,128)(2,1)S(1)} %get-tuple-element.20), channel_id=1, source_target_pairs={{0,4},{4,8},{8,12},{12,16},{16,20},{20,24},{24,28},{1,5},{5,9},{9,... | collective-permute-start | bytes 393224 | tf_op jit(solution)/shard_map/ppermute | solution.py:23
  52.8 20.7 %collective-permute-start.1 = (bf16[2,128,256]{2,1,0:T(8,128)(2,1)S(1)}, bf16[2,128,256]{2,1,0:T(8,128)(2,1)S(1)}, u32[]{:S(2)}, u32[]{:S(2)}) collective-permute-start(bf16[2,128,256]{2,1,0:T(8,128)(2,1)S(1)} %get-tuple-element.20), channel_id=1, source_target_pairs={{0,8},{4,12},{8,16},{12,20},{16,24},{20,28},{1,9},{5,13},{9,17},{1... | collective-permute-start | bytes 393224 | tf_op jit(solution)/shard_map/ppermute | solution.py:23
  56.5 3.5 %copy-start.5 = (bf16[31,256]{1,0:T(8,128)(2,1)S(1)}, bf16[31,256]{1,0:T(8,128)(2,1)}, u32[]{:S(2)}) copy-start(bf16[31,256]{1,0:T(8,128)(2,1)} %param.29) | copy-start | bytes 47620
  56.6 4.9 %collective-permute-start.4 = (bf16[30,256]{1,0:T(8,128)(2,1)S(1)}, bf16[30,256]{1,0:T(8,128)(2,1)S(1)}, u32[]{:S(2)}, u32[]{:S(2)}) collective-permute-start(bf16[30,256]{1,0:T(8,128)(2,1)S(1)} %slice.275), channel_id=1, source_target_pairs={{0,4},{4,8},{8,12},{12,16},{16,20},{20,24},{24,28},{1,5},{5,9},{9,... | collective-permute-start | bytes 46088 | tf_op jit(solution)/shard_map/ppermute | solution.py:23
  73.4 13.5 %copy-start.4 = (f32[1024,256]{1,0:T(8,128)S(1)}, f32[1024,256]{1,0:T(8,128)}, u32[]{:S(2)}) copy-start(f32[1024,256]{1,0:T(8,128)} %get-tuple-element.31) | copy-start | bytes 3145732
  73.7 7.6 %collective-permute-start.2 = (bf16[2,128,256]{2,1,0:T(8,128)(2,1)S(1)}, bf16[2,128,256]{2,1,0:T(8,128)(2,1)S(1)}, u32[]{:S(2)}, u32[]{:S(2)}) collective-permute-start(bf16[2,128,256]{2,1,0:T(8,128)(2,1)S(1)} %get-tuple-element.65), channel_id=1, source_target_pairs={{0,8},{4,12},{8,16},{12,20},{16,24},{20,28},{1,9},{5,13},{9,17},{1... | collective-permute-start | bytes 393224 | tf_op jit(solution)/shard_map/ppermute | solution.py:23
  78.7 8.3 %copy-start.7 = (f32[256]{0:T(256)S(1)}, f32[256]{0:T(256)}, u32[]{:S(2)}) copy-start(f32[256]{0:T(256)} %param.30) | copy-start | bytes 3076
  81.5 7.3 %collective-permute-start.3 = (bf16[2,128,128]{2,1,0:T(8,128)(2,1)S(1)}, bf16[2,128,128]{2,1,0:T(8,128)(2,1)S(1)}, u32[]{:S(2)}, u32[]{:S(2)}) collective-permute-start(bf16[2,128,128]{2,1,0:T(8,128)(2,1)S(1)} %slice.552), channel_id=1, source_target_pairs={{0,16},{4,20},{8,24},{12,28},{1,17},{5,21},{9,25},{13,29},{2,18},{... | collective-permute-start | bytes 196616 | tf_op jit(solution)/shard_map/ppermute | solution.py:23
  86.9 0.7 copy-start.6
  88.8 0.7 copy-start.3
  89.5 1.4 %copy-start.1 = (bf16[256,2048]{1,0:T(8,128)(2,1)S(1)}, bf16[256,2048]{1,0:T(8,128)(2,1)}, u32[]{:S(2)}) copy-start(bf16[256,2048]{1,0:T(8,128)(2,1)} %wd_ref.1) | copy-start | bytes 3145732
  89.5 1.5 %copy-start.2 = (bf16[256,2048]{1,0:T(8,128)(2,1)S(1)}, bf16[256,2048]{1,0:T(8,128)(2,1)}, u32[]{:S(2)}) copy-start(bf16[256,2048]{1,0:T(8,128)(2,1)} %wc_ref.1) | copy-start | bytes 3145732

commit v4 on v2

--- a/solution.py
+++ b/solution.py
@@ -15,12 +15,6 @@
 TINY_NORM = 1e-06
 TINY_VAR = 1e-05
 HIGHEST = lax.Precision.HIGHEST
-
-
-def shifted(block, axis, distance):
-    devices = range(lax.axis_size(axis))
-    route = [(i - distance, i) for i in devices if i - distance in devices]
-    return lax.ppermute(block, axis, route)
 
 
 def nt(a, b):
@@ -157,58 +151,6 @@
     )(query_raw, key_raw, value_raw, gates)
 
 
-def finish_kernel(
-    heads, width, place_ref, all_ref, outa_ref, outb_ref, gate_ref, gain_ref, mixed_ref, carry_s
-):
-    rows = outb_ref.shape[1]
-    carry_s[...] = jnp.zeros_like(carry_s)
-
-    def hop(i, carry):
-        moved = [
-            mm(all_ref[i, h, :, :width], carry_s[h])
-            for h in range(heads)
-        ]
-        for h in range(heads):
-            carry_s[h] = moved[h] + all_ref[i, h, :, width:].astype(jnp.float32)
-        return carry
-
-    lax.fori_loop(0, place_ref[0], hop, 0)
-    tile = 256
-
-    def one(c, carry):
-        at = pl.ds(pl.multiple_of(c * tile, tile), tile)
-        for h in range(heads):
-            lanes = slice(h * width, (h + 1) * width)
-            result = outb_ref[h, at, :] + mm(outa_ref[h, at, :], carry_s[h])
-            result = result * lax.rsqrt(
-                jnp.mean(result * result, axis=-1, keepdims=True) + TINY_NORM
-            )
-            gate = gate_ref[at, lanes].astype(jnp.float32)
-            mixed_ref[at, lanes] = (result * gain_ref[...] * jax.nn.silu(gate)).astype(
-                jnp.bfloat16
-            )
-        return carry
-
-    lax.fori_loop(0, rows // tile, one, 0)
-
-
-def finish(place, states, outa, outb, gate, gain, heads, width):
-    rows = outb.shape[1]
-    vm = pl.BlockSpec(memory_space=pltpu.VMEM)
-    return pl.pallas_call(
-        functools.partial(finish_kernel, heads, width),
-        out_shape=jax.ShapeDtypeStruct((rows, heads * width), jnp.bfloat16),
-        in_specs=[pl.BlockSpec(memory_space=pltpu.SMEM)] + [vm] * 5,
-        out_specs=vm,
-        scratch_shapes=[pltpu.VMEM((heads, width, width), jnp.float32)],
-        compiler_params=pltpu.CompilerParams(vmem_limit_bytes=40 * 1024 * 1024),
-        cost_estimate=pl.CostEstimate(
-            flops=2_000_000_000, bytes_accessed=6_000_000, transcendentals=0
-        ),
-        name="delta_finish",
-    )(place, states, outa, outb, gate, gain)
-
-
 MESH = pl.DeviceIdType.MESH
 
 
@@ -344,6 +286,239 @@
         ),
         name="gather_project",
     )(tokens, *weights, w_gates, rates)
+
+
+def middle_kernel(
+    heads, width, final_ref, gv_ref, gg_ref, cg_ref, taps_ref, ln_gain_ref, ln_shift_ref,
+    outa_ref, outb_ref, dg_ref, gain_ref, mixed_ref, conv_ref,
+    padded, filtered, halo_out, halo_in, sums_out, sums_in, near, window_s, sent_s, far_s,
+    near_send, near_recv, far_send, far_recv, halo_send, halo_recv, ln_send, ln_recv,
+):
+    rows = gv_ref.shape[0]
+    halo = halo_in.shape[0]
+    lanes = padded.shape[2]
+    groups = padded.shape[0]
+    kernel = taps_ref.shape[0]
+    tiles = rows // BLOCK
+    sp, place = lax.axis_size("sp"), lax.axis_index("sp")
+    tp, me = lax.axis_size("tp"), lax.axis_index("tp")
+    reaches = [2]
+    while 2 * reaches[-1] < sp:
+        reaches.append(2 * reaches[-1])
+    distances = [1, 2] + reaches[1:]
+    barrier = pltpu.get_barrier_semaphore()
+    for step in distances:
+        for to in (step, sp - step):
+            pl.semaphore_signal(
+                barrier, inc=1, device_id={"sp": lax.rem(place + to, sp)}, device_id_type=MESH
+            )
+    for step in range(1, tp):
+        pl.semaphore_signal(
+            barrier, inc=1, device_id={"tp": lax.rem(me + step, tp)}, device_id_type=MESH
+        )
+    pl.semaphore_wait(barrier, 2 * len(distances) + tp - 1)
+
+    def onward(src, dst, send, recv, step):
+        return pltpu.make_async_remote_copy(
+            src_ref=src,
+            dst_ref=dst,
+            send_sem=send,
+            recv_sem=recv,
+            device_id={"sp": lax.rem(place + step, sp)},
+            device_id_type=MESH,
+        )
+
+    firsts = [
+        onward(final_ref, near.at[i], near_send.at[i], near_recv.at[i], i + 1) for i in range(2)
+    ]
+    for copy in firsts:
+        copy.start()
+
+    def at(t):
+        return pl.ds(pl.multiple_of(t * BLOCK, BLOCK), BLOCK)
+
+    def unit(t, carry):
+        value = gv_ref[at(t), :].astype(jnp.float32)
+        units = (value * jax.nn.sigmoid(gg_ref[at(t), :].astype(jnp.float32))).astype(jnp.bfloat16)
+        wide = units.astype(jnp.float32)
+        for g in range(groups):
+            padded[g, pl.ds(pl.multiple_of(t * BLOCK + halo, halo), BLOCK), :] = wide[
+                :, g * lanes : (g + 1) * lanes
+            ]
+        return units
+
+    units = unit(tiles - 1, 0)
+    halo_out[...] = units[BLOCK - halo :, :]
+    halo_copy = onward(halo_out, halo_in, halo_send.at[0], halo_recv.at[0], 1)
+    halo_copy.start()
+
+    def unit_loop(t, carry):
+        unit(t, 0)
+        return carry
+
+    lax.fori_loop(0, tiles - 1, unit_loop, 0)
+
+    def conv(t, carry):
+        first = jnp.zeros((BLOCK, 1), jnp.float32)
+        second = jnp.zeros((BLOCK, 1), jnp.float32)
+        for g in range(groups):
+            total = jnp.zeros((BLOCK, lanes), jnp.float32)
+            for j in range(kernel):
+                start = t * BLOCK + (halo - kernel + 1 + j)
+                tap = taps_ref[j : j + 1, g * lanes : (g + 1) * lanes]
+                total = total + padded[g, pl.ds(start, BLOCK), :] * tap
+            filtered[g, at(t), :] = total
+            first = first + jnp.sum(total, axis=1, keepdims=True)
+            second = second + jnp.sum(total * total, axis=1, keepdims=True)
+        lane = lax.broadcasted_iota(jnp.int32, (BLOCK, BLOCK), 1)
+        sums_out[t] = jnp.where(lane == 0, first, jnp.where(lane == 1, second, 0.0)).T[:8, :]
+        return carry
+
+    half = tiles // 2
+    lax.fori_loop(1, half, conv, 0)
+    for copy in firsts:
+        copy.wait()
+    for h in range(heads):
+        one = jnp.where(place >= 1, near[0, h].astype(jnp.float32), 0.0)
+        two = jnp.where(place >= 2, near[1, h].astype(jnp.float32), 0.0)
+        moved = mm(one[:, :width], two)
+        window_s[h] = jnp.concatenate(
+            [moved[:, :width], moved[:, width:] + one[:, width:]], axis=1
+        )
+        sent_s[0, h] = window_s[h].astype(jnp.bfloat16)
+
+    def step_copy(i):
+        return onward(sent_s.at[i], far_s.at[i], far_send.at[i], far_recv.at[i], reaches[i])
+
+    step_copy(0).start()
+    lax.fori_loop(half, tiles, conv, 0)
+    halo_copy.wait()
+    before = jnp.where(place >= 1, halo_in[...].astype(jnp.float32), 0.0)
+    for g in range(groups):
+        padded[g, :halo, :] = before[:, g * lanes : (g + 1) * lanes]
+    conv(0, 0)
+
+    def ln_copy(step):
+        return pltpu.make_async_remote_copy(
+            src_ref=sums_out,
+            dst_ref=sums_in.at[step - 1],
+            send_sem=ln_send.at[step - 1],
+            recv_sem=ln_recv.at[step - 1],
+            device_id={"tp": lax.rem(me + step, tp)},
+            device_id_type=MESH,
+        )
+
+    for step in range(1, tp):
+        ln_copy(step).start()
+    for i in range(len(reaches) - 1):
+        step_copy(i).wait()
+        for h in range(heads):
+            earlier = jnp.where(place >= reaches[i], far_s[i, h].astype(jnp.float32), 0.0)
+            window = window_s[h]
+            moved = mm(window[:, :width], earlier)
+            window_s[h] = jnp.concatenate(
+                [moved[:, :width], moved[:, width:] + window[:, width:]], axis=1
+            )
+            sent_s[i + 1, h] = window_s[h].astype(jnp.bfloat16)
+        step_copy(i + 1).start()
+    for step in range(1, tp):
+        ln_copy(step).wait()
+    channels = groups * lanes * tp
+
+    def norm(t, carry):
+        sums = sums_out[t]
+        for step in range(1, tp):
+            sums = sums + sums_in[step - 1, t]
+        sums = jnp.concatenate([sums, jnp.zeros((BLOCK - 8, BLOCK), jnp.float32)], axis=0).T
+        center = sums[:, 0:1] / channels
+        variance = jnp.maximum(sums[:, 1:2] / channels - center * center, 0.0)
+        scale = lax.rsqrt(variance + TINY_VAR)
+        for g in range(groups):
+            cut = slice(g * lanes, (g + 1) * lanes)
+            normed = (filtered[g, at(t), :] - center) * scale
+            normed = normed * ln_gain_ref[:, cut] + ln_shift_ref[:, cut]
+            gate = cg_ref[at(t), cut].astype(jnp.float32)
+            conv_ref[at(t), cut] = (jax.nn.silu(normed) * jax.nn.silu(gate)).astype(jnp.bfloat16)
+        return carry
+
+    lax.fori_loop(0, tiles, norm, 0)
+    last = len(reaches) - 1
+    step_copy(last).wait()
+    carried = []
+    for h in range(heads):
+        earlier = jnp.where(
+            place >= reaches[last], far_s[last, h, :, width:].astype(jnp.float32), 0.0
+        )
+        window = window_s[h]
+        carried.append((mm(window[:, :width], earlier) + window[:, width:]).astype(jnp.bfloat16))
+
+    def one_tile(t, carry):
+        for h in range(heads):
+            cut = slice(h * width, (h + 1) * width)
+            result = outb_ref[h, at(t), :] + mm(outa_ref[h, at(t), :], carried[h])
+            result = result * lax.rsqrt(
+                jnp.mean(result * result, axis=-1, keepdims=True) + TINY_NORM
+            )
+            gate = dg_ref[at(t), cut].astype(jnp.float32)
+            mixed_ref[at(t), cut] = (result * gain_ref[...] * jax.nn.silu(gate)).astype(
+                jnp.bfloat16
+            )
+        return carry
+
+    lax.fori_loop(0, tiles, one_tile, 0)
+
+
+def middle(final, glu_value, glu_gate, conv_gate, taps, ln_gain, ln_shift, outa, outb, gate, gain):
+    heads, width = final.shape[0], final.shape[1]
+    rows, channels = glu_value.shape
+    kernel = taps.shape[0]
+    halo = (kernel - 1 + 31) // 32 * 32
+    lanes = min(channels, 128)
+    groups = channels // lanes
+    sp, tp = lax.axis_size("sp"), lax.axis_size("tp")
+    steps = 1
+    while 2 ** (steps + 1) < sp:
+        steps += 1
+    vm = pl.BlockSpec(memory_space=pltpu.VMEM)
+    dma = pltpu.SemaphoreType.DMA
+    tiles = rows // BLOCK
+    pair = (heads, width, 2 * width)
+    return pl.pallas_call(
+        functools.partial(middle_kernel, heads, width),
+        out_shape=(
+            jax.ShapeDtypeStruct((rows, heads * width), jnp.bfloat16),
+            jax.ShapeDtypeStruct((rows, channels), jnp.bfloat16),
+        ),
+        in_specs=[vm] * 11,
+        out_specs=(vm, vm),
+        scratch_shapes=[
+            pltpu.VMEM((groups, halo + rows, lanes), jnp.float32),
+            pltpu.VMEM((groups, rows, lanes), jnp.float32),
+            pltpu.VMEM((halo, channels), jnp.bfloat16),
+            pltpu.VMEM((halo, channels), jnp.bfloat16),
+            pltpu.VMEM((tiles, 8, BLOCK), jnp.float32),
+            pltpu.VMEM((tp - 1, tiles, 8, BLOCK), jnp.float32),
+            pltpu.VMEM((2,) + pair, jnp.bfloat16),
+            pltpu.VMEM(pair, jnp.float32),
+            pltpu.VMEM((steps,) + pair, jnp.bfloat16),
+            pltpu.VMEM((steps,) + pair, jnp.bfloat16),
+            dma((2,)),
+            dma((2,)),
+            dma((steps,)),
+            dma((steps,)),
+            dma((1,)),
+            dma((1,)),
+            dma((tp - 1,)),
+            dma((tp - 1,)),
+        ],
+        compiler_params=pltpu.CompilerParams(
+            collective_id=2, has_side_effects=True, vmem_limit_bytes=40 * 1024 * 1024
+        ),
+        cost_estimate=pl.CostEstimate(
+            flops=10_000_000_000, bytes_accessed=20_000_000, transcendentals=0
+        ),
+        name="exchange_middle",
+    )(final, glu_value, glu_gate, conv_gate, taps, ln_gain, ln_shift, outa, outb, gate, gain)
 
 
 def output_kernel(
@@ -492,8 +667,6 @@
     out_delta,
     out_conv,
 ):
-    rows_here = tokens.shape[0]
-    tp_size = lax.axis_size("tp")
     head_size = head_gain.shape[0]
     heads_here = w_query.shape[1] // head_size
     first_head = lax.axis_index("tp") * heads_here
@@ -524,34 +697,18 @@
     outa, outb, final = delta_rule(
         query_raw, key_raw, value_raw, gates, heads_here, head_size
     )
-    states = lax.all_gather(final, "sp")
-    place = lax.axis_index("sp").astype(jnp.int32).reshape(1)
-    delta_mixed = finish(
-        place, states, outa, outb, delta_gate_raw, head_gain[None, :], heads_here, head_size
-    )
-    kernel = conv_taps.shape[0]
-    channels = conv_taps.shape[1]
-    gated_units = (
-        glu_value_raw.astype(jnp.float32) * jax.nn.sigmoid(glu_gate_raw.astype(jnp.float32))
-    ).astype(jnp.bfloat16)
-    before = shifted(gated_units[rows_here - (kernel - 1) :], "sp", 1)
-    padded = jnp.concatenate([before, gated_units], axis=0)
-    filtered = jnp.zeros((rows_here, channels), jnp.float32)
-    for offset in range(kernel):
-        filtered = filtered + padded[offset : offset + rows_here].astype(jnp.float32) * conv_taps[
-            offset
-        ].astype(jnp.float32)
-    first_sum = jnp.sum(filtered, axis=1)
-    second_sum = jnp.sum(filtered * filtered, axis=1)
-    first_sum, second_sum = lax.psum((first_sum, second_sum), "tp")
-    channels_all = channels * tp_size
-    center = first_sum / channels_all
-    variance = jnp.maximum(second_sum / channels_all - center * center, 0.0)
-    normed = (filtered - center[:, None]) * lax.rsqrt(variance + TINY_VAR)[
-        :, None
-    ] * ln_gain + ln_shift
-    conv_mixed = (jax.nn.silu(normed) * jax.nn.silu(conv_gate_raw.astype(jnp.float32))).astype(
-        jnp.bfloat16
+    delta_mixed, conv_mixed = middle(
+        final,
+        glu_value_raw,
+        glu_gate_raw,
+        conv_gate_raw,
+        conv_taps.astype(jnp.float32),
+        ln_gain[None, :],
+        ln_shift[None, :],
+        outa,
+        outb,
+        delta_gate_raw,
+        head_gain[None, :],
     )
     return output_projection(delta_mixed, conv_mixed, out_delta, out_conv)
 

time: 140 us -> 104 us (0.74)
  waiting for transfers between devices: 23.8 us -> 0 us
  Pallas kernels: 76.9 us -> 99.1 us
  between operations: 13.6 us -> 0.14 us
  other arithmetic: 8.55 us -> 0.41 us
  blocking collectives: 7.62 us -> 0 us
  starting transfers between devices: 2.89 us -> 0 us
  local copies, waits for them, and re-layouts: 6.42 us -> 3.56 us
    all_gather x1 -> x0, waiting for transfers between devices: 23.8 us -> none  [local(): states = lax.all_gather(final, 'sp')]
    pallas_call x1, Pallas kernels: 1.22 us -> 24.3 us  [middle(): pl.pallas_call(functools.partial(middle_kernel, heads, width), out_shape=...]
    psum x1 -> x0, blocking collectives: 7.62 us -> none  [local(): first_sum, second_sum = lax.psum((first_sum, second_sum), 'tp')]
    reduce_sum x1 -> x0, other arithmetic: 5.96 us -> none  [local(): first_sum = jnp.sum(filtered, axis=1)]
    ppermute x1 -> x0, starting transfers between devices: 2.89 us -> none  [shifted(): return lax.ppermute(block, axis, route)]
    unnamed x21 -> x19, local copies, waits for them, and re-layouts: 5.46 us -> 2.61 us
    convert_element_type x2 -> x1, other arithmetic: 2.15 us -> 0.01 us  [local(): conv_taps.astype(jnp.float32)]
  transfers between devices with their start and end apart: 2 -> 0, of which waited for: 1 -> 0; matrix products, arithmetic and copies ran while one was open for 6% -> 0% of each run, Pallas kernels for 10% -> 0%
where the time goes in v4:
time: 104 us; the launch traced here: 103 us
  Pallas kernels  99.1 us (95%)
  local copies, waits for them, and re-layouts  3.56 us (3%)
    pallas_call x1, Pallas kernels, project(): pl.pallas_call(functools.partial(project_kernel, heads), out_shape=tuple(...  33.5 us
    pallas_call x1, Pallas kernels, output_projection(): pl.pallas_call(output_kernel, out_shape=jax.ShapeDtypeStruct((rows, width...  27.3 us
    pallas_call x1, Pallas kernels, middle(): pl.pallas_call(functools.partial(middle_kernel, heads, width), out_shape=...  24.3 us
    pallas_call x1, Pallas kernels, delta_rule(): pl.pallas_call(functools.partial(delta_kernel, heads, width), out_shape=(...  14 us
    unnamed x19, local copies, waits for them, and re-layouts  2.61 us

profile of v4, /device:TPU:0, one launch (start us, length us, event | category | flops | bytes accessed | tf_op | source)
XLA Modules:
  0.0 103.2 jit_solution(5140723852500426098)
XLA Ops:
  0.0 0.8 constant_dynamic-slice_fusion
  0.8 0.3 copy.20
  1.1 0.0 copy-start
  1.1 0.3 copy.21
  1.4 0.1 pad.5.clone
  1.5 0.0 copy-start.7
  1.5 0.3 maximum_maximum_fusion.refs_8_
  1.9 0.3 copy-done.7
  2.2 0.1 dynamic-slice_exponential_fusion
  2.3 0.1 maximum_bitcast_fusion.refs_9_
  2.3 0.0 copy-done
  2.3 33.5 %gather_project.1 = (bf16[1024,256]{1,0:T(8,128)(2,1)S(1)}, bf16[1024,256]{1,0:T(8,128)(2,1)S(1)}, bf16[1024,256]{1,0:T(8,128)(2,1)S(1)}, bf16[1024,256]{1,0:T(8...) custom-call(bf16[1024,512]{1,0:T(8,128)(2,1)S(1)} %copy-done, ...), custom_call_target="tpu_custom_call" | custom-call | flops 10000000000 | bytes 20000000 | tf_op jit(solution)/shard_map/gather_project/pallas_call | solution.py:264
  35.9 0.0 copy-start.6
  35.9 0.0 copy-start.4
  35.9 14.0 %delta_rule.1 = (bf16[2,1024,128]{2,1,0:T(8,128)(2,1)S(1)}, f32[2,1024,128]{2,1,0:T(8,128)S(1)}, bf16[2,128,256]{2,1,0:T(8,128)(2,1)S(1)}) custom-call(bf16[1024,256]{1,0:T(8,128)(2,1)S(1)} %get-tuple-element.18.q_ref, bf16[1024,256]{1,0:T(8,128)(2,1)S(1)} %get-tuple-element.19.k_ref, bf16[1024,256]{1,0:T(8,128)(2,1)S(1)} %get-tuple-element.20.v_ref, ...), custom_call_target="tpu_custom_call" | custom-call | flops 10000000000 | bytes 4000000 | tf_op jit(solution)/shard_map/delta_rule/pallas_call | solution.py:127
  49.9 0.0 copy-done.6
  49.9 0.0 copy-start.3
  49.9 0.0 copy-start.5
  49.9 0.0 copy-done.4
  49.9 0.6 copy-done.3
  50.6 0.0 copy-done.5
  50.6 0.0 copy-start.1
  50.6 0.0 copy-start.2
  50.6 24.3 %exchange_middle.1 = (bf16[1024,256]{1,0:T(8,128)(2,1)S(1)}, bf16[1024,256]{1,0:T(8,128)(2,1)S(1)}) custom-call(bf16[2,128,256]{2,1,0:T(8,128)(2,1)S(1)} %get-tuple-element.22.final_ref, bf16[1024,256]{1,0:T(8,128)(2,1)S(1)} %get-tuple-element.23.gv_ref, bf16[1024,256]{1,0:T(8,128)(2,1)S(1)} %get-tuple-element.24.gg_ref, ...), custom_call_target="tpu_custom_call" | custom-call | flops 10000000000 | bytes 20000000 | tf_op jit(solution)/shard_map/exchange_middle/pallas_call | solution.py:486
  74.9 0.0 copy-done.1
  74.9 0.0 copy-done.2
  74.9 27.3 %output_scatter.1 = bf16[256,2048]{1,0:T(8,128)(2,1)S(1)} custom-call(bf16[1024,256]{1,0:T(8,128)(2,1)S(1)} %get-tuple-element.29.dm_ref, bf16[1024,256]{1,0:T(8,128)(2,1)S(1)} %get-tuple-element.30.cm_ref, bf16[256,2048]{1,0:T(8,128)(2,1)S(1)} %copy-done.1, bf16[256,2048]{1,0:T(8,128)(2,1)S(1)} %copy-done.2), custom_call_target="tpu_custom_call" | custom-call | flops 10000000000 | bytes 20000000 | tf_op jit(solution)/shard_map/output_scatter/pallas_call | solution.py:626
  102.2 1.0 copy.23
  (4 shorter events, 0.0 us)
Async XLA Ops:
  1.1 1.2 %copy-start = (bf16[1024,512]{1,0:T(8,128)(2,1)S(1)}, bf16[1024,512]{1,0:T(8,128)(2,1)}, u32[]{:S(2)}) copy-start(bf16[1024,512]{1,0:T(8,128)(2,1)} %refs_0_.1) | copy-start | bytes 3145732
  1.5 0.7 copy-start.7
  35.9 14.0 %copy-start.6 = (bf16[31,256]{1,0:T(8,128)(2,1)S(1)}, bf16[31,256]{1,0:T(8,128)(2,1)}, u32[]{:S(2)}) copy-start(bf16[31,256]{1,0:T(8,128)(2,1)} %param.29) | copy-start | bytes 47620
  35.9 14.0 %copy-start.4 = (f32[256]{0:T(256)S(1)}, f32[256]{0:T(256)}, u32[]{:S(2)}) copy-start(f32[256]{0:T(256)} %param.31) | copy-start | bytes 3076
  49.9 0.7 copy-start.3
  49.9 0.7 copy-start.5
  50.6 24.3 %copy-start.1 = (bf16[256,2048]{1,0:T(8,128)(2,1)S(1)}, bf16[256,2048]{1,0:T(8,128)(2,1)}, u32[]{:S(2)}) copy-start(bf16[256,2048]{1,0:T(8,128)(2,1)} %wd_ref.1) | copy-start | bytes 3145732
  50.6 24.3 %copy-start.2 = (bf16[256,2048]{1,0:T(8,128)(2,1)S(1)}, bf16[256,2048]{1,0:T(8,128)(2,1)}, u32[]{:S(2)}) copy-start(bf16[256,2048]{1,0:T(8,128)(2,1)} %wc_ref.1) | copy-start | bytes 3145732

commit v5 on v4

--- a/solution.py
+++ b/solution.py
@@ -8,8 +8,8 @@
 from jax.sharding import PartitionSpec as P
 
 BLOCK = 128
-CHUNKS = 4
-CUTS = 4
+CHUNKS = 8
+CUTS = 8
 
 
 TINY_NORM = 1e-06
@@ -172,9 +172,10 @@
 
 def project_kernel(heads, *refs):
     count = 7
-    tok_ref, w_refs, wg_ref, rate_ref = refs[0], refs[1 : 1 + count], refs[8], refs[9]
+    tok_ref, far_refs, wg_ref, rate_ref = refs[0], refs[1 : 1 + count], refs[8], refs[9]
     out_refs, gates_ref = refs[10 : 10 + count], refs[17]
-    full, y_send, y_recv, own_send, own_recv, fwd_send, fwd_recv = refs[18:]
+    full, y_send, y_recv, own_send, own_recv, fwd_send, fwd_recv, w_sem = refs[18:26]
+    w_refs = refs[26:]
     rows, part = tok_ref.shape
     step = rows // CHUNKS
     chips, me, core, chip, sibling = sharded_place()
@@ -222,32 +223,46 @@
     for r in range(CHUNKS):
         for o in range(1, chips):
             across(o, r).start()
+    loads = [
+        pltpu.make_async_copy(far, w_ref, w_sem.at[i])
+        for i, (far, w_ref) in enumerate(zip(far_refs, w_refs))
+    ]
+    for load in loads:
+        load.start()
     for r in range(CHUNKS):
         beside(r).start()
     full[:, columns(me)] = tok_ref[...]
 
-    def chunk(r, carry):
-        for o in range(1, chips):
-            across(o, r).wait_recv()
-            forward(o, r).start()
-        beside(r).wait_recv()
-        for o in range(1, chips):
-            forward(o, r).wait_recv()
-        squares = jnp.zeros((step, 1), jnp.float32)
+    def chunk(first, pieces, carry):
+        for i in range(pieces):
+            for o in range(1, chips):
+                across(o, first + i).wait_recv()
+                forward(o, first + i).start()
+        for i in range(pieces):
+            beside(first + i).wait_recv()
+            for o in range(1, chips):
+                forward(o, first + i).wait_recv()
+        size = step * pieces
+        here = pl.ds(pl.multiple_of(first * step, step), size)
+        squares = jnp.zeros((size, 1), jnp.float32)
         for b in range(2 * chips):
-            piece = full[at(r), b * part : (b + 1) * part].astype(jnp.float32)
+            piece = full[here, b * part : (b + 1) * part].astype(jnp.float32)
             squares = squares + jnp.sum(piece * piece, axis=1, keepdims=True)
         inv_rms = lax.rsqrt(squares / (part * 2 * chips) + TINY_NORM)
         for w_ref, out_ref in zip(w_refs, out_refs):
-            summed = jnp.dot(full[at(r), :], w_ref[...], preferred_element_type=jnp.float32)
-            out_ref[at(r), :] = (summed * inv_rms).astype(jnp.bfloat16)
-        raw = jnp.dot(full[at(r), :], wg_ref[...], preferred_element_type=jnp.float32) * inv_rms
+            summed = jnp.dot(full[here, :], w_ref[...], preferred_element_type=jnp.float32)
+            out_ref[here, :] = (summed * inv_rms).astype(jnp.bfloat16)
+        raw = jnp.dot(full[here, :], wg_ref[...], preferred_element_type=jnp.float32) * inv_rms
         lane = lax.broadcasted_iota(jnp.int32, raw.shape, 1)
         softplus = jnp.maximum(raw, 0.0) + jnp.log1p(jnp.exp(-jnp.abs(raw)))
-        gates_ref[at(r), :] = jnp.where(lane < heads, jax.nn.sigmoid(raw), -rate_ref[...] * softplus)
-        return carry
-
-    lax.fori_loop(0, CHUNKS, chunk, 0)
+        gates_ref[here, :] = jnp.where(lane < heads, jax.nn.sigmoid(raw), -rate_ref[...] * softplus)
+        return carry
+
+    for load in loads:
+        load.wait()
+    paired = CHUNKS // 2 - 1
+    lax.fori_loop(0, paired, lambda r, carry: chunk(2 * r, 2, carry), 0)
+    lax.fori_loop(2 * paired, CHUNKS, lambda r, carry: chunk(r, 1, carry), 0)
     for r in range(CHUNKS):
         for o in range(1, chips):
             across(o, r).wait_send()
@@ -267,7 +282,7 @@
             jax.ShapeDtypeStruct((rows, w.shape[1]), jnp.bfloat16) for w in weights
         )
         + (jax.ShapeDtypeStruct((rows, w_gates.shape[1]), jnp.float32),),
-        in_specs=[vm] * (3 + len(weights)),
+        in_specs=[vm] + [pl.BlockSpec(memory_space=pl.ANY)] * len(weights) + [vm] * 2,
         out_specs=(vm,) * (1 + len(weights)),
         scratch_shapes=[
             pltpu.VMEM((rows, part * tp), jnp.bfloat16),
@@ -277,7 +292,9 @@
             dma((CHUNKS,)),
             dma((others, CHUNKS)),
             dma((others, CHUNKS)),
-        ],
+            dma((len(weights),)),
+        ]
+        + [pltpu.VMEM(w.shape, w.dtype) for w in weights],
         compiler_params=pltpu.CompilerParams(
             collective_id=0, has_side_effects=True, vmem_limit_bytes=48 * 1024 * 1024
         ),

time: 104 us -> 101 us (0.971)
  Pallas kernels: 99.1 us -> 96.3 us
    pallas_call x1, Pallas kernels: 33.5 us -> 29.7 us  [project(): pl.pallas_call(functools.partial(project_kernel, heads), out_shape=tuple(...]
where the time goes in v5:
time: 101 us; the launch traced here: 100 us
  Pallas kernels  96.3 us (95%)
  local copies, waits for them, and re-layouts  3.56 us (4%)
    pallas_call x1, Pallas kernels, project(): pl.pallas_call(functools.partial(project_kernel, heads), out_shape=tuple(...  29.7 us
    pallas_call x1, Pallas kernels, output_projection(): pl.pallas_call(output_kernel, out_shape=jax.ShapeDtypeStruct((rows, width...  27.5 us
    pallas_call x1, Pallas kernels, middle(): pl.pallas_call(functools.partial(middle_kernel, heads, width), out_shape=...  25.1 us
    pallas_call x1, Pallas kernels, delta_rule(): pl.pallas_call(functools.partial(delta_kernel, heads, width), out_shape=(...  14 us
    unnamed x19, local copies, waits for them, and re-layouts  2.61 us

profile of v5, /device:TPU:0, one launch (start us, length us, event | category | flops | bytes accessed | tf_op | source)
XLA Modules:
  0.0 100.4 jit_solution(7189337954869972130)
XLA Ops:
  0.0 0.8 constant_dynamic-slice_fusion
  0.8 0.3 copy.20
  1.1 0.0 copy-start
  1.1 0.3 copy.21
  1.4 0.1 pad.5.clone
  1.5 0.0 copy-start.7
  1.5 0.3 maximum_maximum_fusion.refs_8_
  1.9 0.3 copy-done.7
  2.2 0.1 dynamic-slice_exponential_fusion
  2.3 0.1 maximum_bitcast_fusion.refs_9_
  2.3 0.0 copy-done
  2.3 29.7 %gather_project.1 = (bf16[1024,256]{1,0:T(8,128)(2,1)S(1)}, bf16[1024,256]{1,0:T(8,128)(2,1)S(1)}, bf16[1024,256]{1,0:T(8,128)(2,1)S(1)}, bf16[1024,256]{1,0:T(8...) custom-call(bf16[1024,512]{1,0:T(8,128)(2,1)S(1)} %copy-done, ...), custom_call_target="tpu_custom_call" | custom-call | flops 10000000000 | bytes 20000000 | tf_op jit(solution)/shard_map/gather_project/pallas_call | solution.py:279
  32.0 0.0 copy-start.6
  32.0 0.0 copy-start.4
  32.0 14.0 %delta_rule.1 = (bf16[2,1024,128]{2,1,0:T(8,128)(2,1)S(1)}, f32[2,1024,128]{2,1,0:T(8,128)S(1)}, bf16[2,128,256]{2,1,0:T(8,128)(2,1)S(1)}) custom-call(bf16[1024,256]{1,0:T(8,128)(2,1)S(1)} %get-tuple-element.18.q_ref, bf16[1024,256]{1,0:T(8,128)(2,1)S(1)} %get-tuple-element.19.k_ref, bf16[1024,256]{1,0:T(8,128)(2,1)S(1)} %get-tuple-element.20.v_ref, ...), custom_call_target="tpu_custom_call" | custom-call | flops 10000000000 | bytes 4000000 | tf_op jit(solution)/shard_map/delta_rule/pallas_call | solution.py:127
  46.0 0.0 copy-done.6
  46.0 0.0 copy-start.3
  46.1 0.0 copy-start.5
  46.1 0.0 copy-done.4
  46.1 0.6 copy-done.3
  46.7 0.0 copy-done.5
  46.7 0.0 copy-start.1
  46.7 0.0 copy-start.2
  46.7 25.1 %exchange_middle.1 = (bf16[1024,256]{1,0:T(8,128)(2,1)S(1)}, bf16[1024,256]{1,0:T(8,128)(2,1)S(1)}) custom-call(bf16[2,128,256]{2,1,0:T(8,128)(2,1)S(1)} %get-tuple-element.22.final_ref, bf16[1024,256]{1,0:T(8,128)(2,1)S(1)} %get-tuple-element.23.gv_ref, bf16[1024,256]{1,0:T(8,128)(2,1)S(1)} %get-tuple-element.24.gg_ref, ...), custom_call_target="tpu_custom_call" | custom-call | flops 10000000000 | bytes 20000000 | tf_op jit(solution)/shard_map/exchange_middle/pallas_call | solution.py:503
  71.9 0.0 copy-done.1
  71.9 0.0 copy-done.2
  71.9 27.5 %output_scatter.1 = bf16[256,2048]{1,0:T(8,128)(2,1)S(1)} custom-call(bf16[1024,256]{1,0:T(8,128)(2,1)S(1)} %get-tuple-element.29.dm_ref, bf16[1024,256]{1,0:T(8,128)(2,1)S(1)} %get-tuple-element.30.cm_ref, bf16[256,2048]{1,0:T(8,128)(2,1)S(1)} %copy-done.1, bf16[256,2048]{1,0:T(8,128)(2,1)S(1)} %copy-done.2), custom_call_target="tpu_custom_call" | custom-call | flops 10000000000 | bytes 20000000 | tf_op jit(solution)/shard_map/output_scatter/pallas_call | solution.py:643
  99.4 1.0 copy.23
  (4 shorter events, 0.0 us)
Async XLA Ops:
  1.1 1.2 %copy-start = (bf16[1024,512]{1,0:T(8,128)(2,1)S(1)}, bf16[1024,512]{1,0:T(8,128)(2,1)}, u32[]{:S(2)}) copy-start(bf16[1024,512]{1,0:T(8,128)(2,1)} %refs_0_.1) | copy-start | bytes 3145732
  1.5 0.7 copy-start.7
  32.0 14.0 %copy-start.6 = (bf16[31,256]{1,0:T(8,128)(2,1)S(1)}, bf16[31,256]{1,0:T(8,128)(2,1)}, u32[]{:S(2)}) copy-start(bf16[31,256]{1,0:T(8,128)(2,1)} %param.29) | copy-start | bytes 47620
  32.0 14.0 %copy-start.4 = (f32[256]{0:T(256)S(1)}, f32[256]{0:T(256)}, u32[]{:S(2)}) copy-start(f32[256]{0:T(256)} %param.31) | copy-start | bytes 3076
  46.0 0.7 copy-start.3
  46.1 0.7 copy-start.5
  46.7 25.2 %copy-start.1 = (bf16[256,2048]{1,0:T(8,128)(2,1)S(1)}, bf16[256,2048]{1,0:T(8,128)(2,1)}, u32[]{:S(2)}) copy-start(bf16[256,2048]{1,0:T(8,128)(2,1)} %wd_ref.1) | copy-start | bytes 3145732
  46.7 25.2 %copy-start.2 = (bf16[256,2048]{1,0:T(8,128)(2,1)S(1)}, bf16[256,2048]{1,0:T(8,128)(2,1)}, u32[]{:S(2)}) copy-start(bf16[256,2048]{1,0:T(8,128)(2,1)} %wc_ref.1) | copy-start | bytes 3145732

commit v6 on v5

--- a/solution.py
+++ b/solution.py
@@ -9,6 +9,7 @@
 
 BLOCK = 128
 CHUNKS = 8
+TOGETHER = 4
 CUTS = 8
 
 
@@ -73,7 +74,7 @@
         return at, c, chains
 
     def pair(p, carry):
-        prepared = [prepare(p * 2 + i) for i in range(2)]
+        prepared = [prepare(p * TOGETHER + i) for i in range(TOGETHER)]
         size = 2
         while size < BLOCK:
             level = (differ >= size) & (differ < 2 * size)
@@ -91,7 +92,7 @@
                 lhs_s[h, c, :BLOCK, :] = solved[:, width:].astype(jnp.bfloat16)
         return carry
 
-    lax.fori_loop(0, blocks // 2, pair, 0)
+    lax.fori_loop(0, blocks // TOGETHER, pair, 0)
     for h in range(heads):
         state_ref[h] = jnp.concatenate([eye, jnp.zeros((width, width), jnp.float32)], axis=1)
 

time: 101 us -> 97.3 us (0.963)
  Pallas kernels: 96.3 us -> 92.4 us
    pallas_call x1, Pallas kernels: 14 us -> 10.1 us  [delta_rule(): pl.pallas_call(functools.partial(delta_kernel, heads, width), out_shape=(...]
where the time goes in v6:
time: 97.3 us; the launch traced here: 96.5 us
  Pallas kernels  92.4 us (95%)
  local copies, waits for them, and re-layouts  3.56 us (4%)
    pallas_call x1, Pallas kernels, project(): pl.pallas_call(functools.partial(project_kernel, heads), out_shape=tuple(...  29.7 us
    pallas_call x1, Pallas kernels, output_projection(): pl.pallas_call(output_kernel, out_shape=jax.ShapeDtypeStruct((rows, width...  27.5 us
    pallas_call x1, Pallas kernels, middle(): pl.pallas_call(functools.partial(middle_kernel, heads, width), out_shape=...  25.1 us
    pallas_call x1, Pallas kernels, delta_rule(): pl.pallas_call(functools.partial(delta_kernel, heads, width), out_shape=(...  10.1 us
    unnamed x19, local copies, waits for them, and re-layouts  2.61 us

profile of v6, /device:TPU:0, one launch (start us, length us, event | category | flops | bytes accessed | tf_op | source)
XLA Modules:
  0.0 96.5 jit_solution(6877952134757687643)
XLA Ops:
  0.0 0.8 constant_dynamic-slice_fusion
  0.8 0.3 copy.20
  1.1 0.0 copy-start
  1.1 0.3 copy.21
  1.4 0.1 pad.5.clone
  1.5 0.0 copy-start.7
  1.5 0.3 maximum_maximum_fusion.refs_8_
  1.9 0.3 copy-done.7
  2.2 0.1 dynamic-slice_exponential_fusion
  2.3 0.1 maximum_bitcast_fusion.refs_9_
  2.3 0.0 copy-done
  2.3 29.7 %gather_project.1 = (bf16[1024,256]{1,0:T(8,128)(2,1)S(1)}, bf16[1024,256]{1,0:T(8,128)(2,1)S(1)}, bf16[1024,256]{1,0:T(8,128)(2,1)S(1)}, bf16[1024,256]{1,0:T(8...) custom-call(bf16[1024,512]{1,0:T(8,128)(2,1)S(1)} %copy-done, ...), custom_call_target="tpu_custom_call" | custom-call | flops 10000000000 | bytes 20000000 | tf_op jit(solution)/shard_map/gather_project/pallas_call | solution.py:280
  32.0 0.0 copy-start.6
  32.0 0.0 copy-start.4
  32.0 10.1 %delta_rule.1 = (bf16[2,1024,128]{2,1,0:T(8,128)(2,1)S(1)}, f32[2,1024,128]{2,1,0:T(8,128)S(1)}, bf16[2,128,256]{2,1,0:T(8,128)(2,1)S(1)}) custom-call(bf16[1024,256]{1,0:T(8,128)(2,1)S(1)} %get-tuple-element.18.q_ref, bf16[1024,256]{1,0:T(8,128)(2,1)S(1)} %get-tuple-element.19.k_ref, bf16[1024,256]{1,0:T(8,128)(2,1)S(1)} %get-tuple-element.20.v_ref, ...), custom_call_target="tpu_custom_call" | custom-call | flops 10000000000 | bytes 4000000 | tf_op jit(solution)/shard_map/delta_rule/pallas_call | solution.py:128
  42.2 0.0 copy-done.6
  42.2 0.0 copy-start.3
  42.2 0.0 copy-start.5
  42.2 0.0 copy-done.4
  42.2 0.6 copy-done.3
  42.9 0.0 copy-done.5
  42.9 0.0 copy-start.1
  42.9 0.0 copy-start.2
  42.9 25.1 %exchange_middle.1 = (bf16[1024,256]{1,0:T(8,128)(2,1)S(1)}, bf16[1024,256]{1,0:T(8,128)(2,1)S(1)}) custom-call(bf16[2,128,256]{2,1,0:T(8,128)(2,1)S(1)} %get-tuple-element.22.final_ref, bf16[1024,256]{1,0:T(8,128)(2,1)S(1)} %get-tuple-element.23.gv_ref, bf16[1024,256]{1,0:T(8,128)(2,1)S(1)} %get-tuple-element.24.gg_ref, ...), custom_call_target="tpu_custom_call" | custom-call | flops 10000000000 | bytes 20000000 | tf_op jit(solution)/shard_map/exchange_middle/pallas_call | solution.py:504
  68.0 0.0 copy-done.1
  68.0 0.0 copy-done.2
  68.0 27.5 %output_scatter.1 = bf16[256,2048]{1,0:T(8,128)(2,1)S(1)} custom-call(bf16[1024,256]{1,0:T(8,128)(2,1)S(1)} %get-tuple-element.29.dm_ref, bf16[1024,256]{1,0:T(8,128)(2,1)S(1)} %get-tuple-element.30.cm_ref, bf16[256,2048]{1,0:T(8,128)(2,1)S(1)} %copy-done.1, bf16[256,2048]{1,0:T(8,128)(2,1)S(1)} %copy-done.2), custom_call_target="tpu_custom_call" | custom-call | flops 10000000000 | bytes 20000000 | tf_op jit(solution)/shard_map/output_scatter/pallas_call | solution.py:644
  95.6 1.0 %copy.23 = bf16[256,2048]{1,0:T(8,128)(2,1)} copy(bf16[256,2048]{1,0:T(8,128)(2,1)S(1)} %output_scatter.1) | data formatting | bytes 2097152
  (4 shorter events, 0.0 us)
Async XLA Ops:
  1.1 1.2 %copy-start = (bf16[1024,512]{1,0:T(8,128)(2,1)S(1)}, bf16[1024,512]{1,0:T(8,128)(2,1)}, u32[]{:S(2)}) copy-start(bf16[1024,512]{1,0:T(8,128)(2,1)} %refs_0_.1) | copy-start | bytes 3145732
  1.5 0.7 copy-start.7
  32.0 10.1 %copy-start.6 = (bf16[31,256]{1,0:T(8,128)(2,1)S(1)}, bf16[31,256]{1,0:T(8,128)(2,1)}, u32[]{:S(2)}) copy-start(bf16[31,256]{1,0:T(8,128)(2,1)} %param.29) | copy-start | bytes 47620
  32.0 10.2 %copy-start.4 = (f32[256]{0:T(256)S(1)}, f32[256]{0:T(256)}, u32[]{:S(2)}) copy-start(f32[256]{0:T(256)} %param.31) | copy-start | bytes 3076
  42.2 0.7 copy-start.3
  42.2 0.7 copy-start.5
  42.9 25.2 %copy-start.1 = (bf16[256,2048]{1,0:T(8,128)(2,1)S(1)}, bf16[256,2048]{1,0:T(8,128)(2,1)}, u32[]{:S(2)}) copy-start(bf16[256,2048]{1,0:T(8,128)(2,1)} %wd_ref.1) | copy-start | bytes 3145732
  42.9 25.2 %copy-start.2 = (bf16[256,2048]{1,0:T(8,128)(2,1)S(1)}, bf16[256,2048]{1,0:T(8,128)(2,1)}, u32[]{:S(2)}) copy-start(bf16[256,2048]{1,0:T(8,128)(2,1)} %wc_ref.1) | copy-start | bytes 3145732
